TPU v7x, 1024 devices: a whole 4x8x16 slice. The times are simulated.
1024 devices in a mesh: ep: 32 (over z, core), tp: 32 (over y, x).
Axes of the slice: x: 4, y: 8, z: 16, core: 2. Of those that a mesh axis runs over, the one named last changes fastest.
Arguments:
- tokens: bfloat16 [2048, 2048], P('ep', 'tp'), may hold values from -6 to 6
- gain_mix: float32 [2048], replicated, may hold values from 0.1 to 1.9
- w_in: bfloat16 [2048, 1024], P(None, 'tp'), may hold values from -0.125 to 0.125
- decay_rate: float32 [64, 64], P('tp'), may hold values from 0.05 to 3
- frequency: float32 [64, 64], P('tp'), may hold values from -3 to 3
- log_step: float32 [64], P('tp'), may hold values from -3 to 0
- input_real: float32 [64, 64, 16], P('tp'), may hold values from -1 to 1
- input_imag: float32 [64, 64, 16], P('tp'), may hold values from -1 to 1
- readout_real: float32 [64, 16, 64], P('tp'), may hold values from -0.75 to 0.75
- readout_imaginary: float32 [64, 16, 64], P('tp'), may hold values from -0.75 to 0.75
- passthrough_scale: float32 [1024], P('tp'), may hold values from -4 to 4
- state_real: float32 [2048, 64, 64], P('ep', 'tp'), may hold values from -4 to 4
- state_imag: float32 [2048, 64, 64], P('ep', 'tp'), may hold values from -4 to 4
- w_out: bfloat16 [1024, 2048], replicated, may hold values from -0.1875 to 0.1875
- gain_ffn: float32 [2048], replicated, may hold values from 0.1 to 1.9
- expert_choice: int32 [2048, 2], P('ep'), may hold values from 0 to 31, all different within a row; in each aligned block of 64 rows (0 to 63, 64 to 127, ...) at most 8 rows name the same one
- expert_weight: float32 [2048, 2], P('ep'), may hold values from 0.2 to 1
- w_gate: bfloat16 [32, 2048, 8192], P('ep', None, 'tp'), may hold values from -0.125 to 0.125
- w_up: bfloat16 [32, 2048, 8192], P('ep', None, 'tp'), may hold values from -0.125 to 0.125
- w_down: bfloat16 [32, 8192, 2048], P('ep', 'tp'), may hold values from -0.0625 to 0.0625
Outputs:
- layer_out: bfloat16 [2048, 2048], P('ep', 'tp')
- next_state_real: float32 [2048, 64, 64], P('ep', 'tp')
- next_state_imaginary: float32 [2048, 64, 64], P('ep', 'tp')
Inputs may be any that keep to these rules, and one draw needn't show every extreme that they name: `expert_choice`: each row names 2 different experts; in the rows of one index of ep (aligned blocks of 64 rows) no expert is named more than 8 times, a bound that some block reaches.
All inputs are finite; a program needn't handle non-finite values.
Results may differ from a plain program's by a relative error of at most 0.017.
Values may be sent and summed in bfloat16 or wider, within the bound.
No kernel may reach another device: no remote copies, remote signals or barrier semaphores. Data moves between devices by JAX's collectives and lax.ppermute only.
A program may use at most 32 MiB of HBM per device.

v0:
```python
import jax
import jax.numpy as jnp
from jax import lax
from jax.sharding import PartitionSpec as P


def sent_to_all(value, axis):
    copies = jnp.broadcast_to(value, (lax.axis_size(axis), *value.shape))
    return lax.all_to_all(copies, axis, split_axis=0, concat_axis=0, tiled=True)


def in_order(parts, dim):
    parts = jnp.moveaxis(parts, 0, dim)
    lengths = parts.shape
    return parts.reshape(*lengths[:dim], lengths[dim] * lengths[dim + 1], *lengths[dim + 2 :])


def gathered_copies(value, axis, dim):
    parts = sent_to_all(value, axis)
    return in_order(parts, dim)


def over_copies(value, axis):
    everything = sent_to_all(value, axis)
    return jnp.sum(everything, axis=0)


def split_up(value, dim, peers):
    before, after = (value.shape[:dim], value.shape[dim + 1 :])
    return jnp.moveaxis(value.reshape(*before, peers, -1, *after), dim, 0)


def summed_on_arrival(value, axis, dim):
    parts = split_up(value, dim, lax.axis_size(axis))
    arrived = lax.all_to_all(parts, axis, split_axis=0, concat_axis=0, tiled=True)
    return arrived.astype(jnp.float32).sum(axis=0)


def rms_norm(values, gains):
    float_values = values.astype(jnp.float32)
    scale = lax.rsqrt(jnp.mean(float_values * float_values, axis=-1, keepdims=True) + 1e-06)
    return (float_values * scale * gains).astype(jnp.bfloat16)


def state_step(
    drive,
    real_state,
    imag_state,
    decay_rate,
    frequency,
    log_step,
    input_real,
    input_imag,
    readout_real,
    readout_imaginary,
    passthrough_scale,
):
    count_of_groups, count_of_channels = (input_real.shape[0], input_real.shape[2])
    step = jnp.exp(log_step)[:, None]
    lam_real = -decay_rate
    magnitude = jnp.exp(lam_real * step)
    abar_real = magnitude * jnp.cos(frequency * step)
    abar_imag = magnitude * jnp.sin(frequency * step)
    denom = lam_real * lam_real + frequency * frequency
    numer = abar_real - 1.0
    factor_real = (numer * lam_real + abar_imag * frequency) / denom
    factor_imag = (abar_imag * lam_real - numer * frequency) / denom
    bbar_real = factor_real[..., None] * input_real - factor_imag[..., None] * input_imag
    bbar_imag = factor_real[..., None] * input_imag + factor_imag[..., None] * input_real
    float_values = drive.astype(jnp.float32).reshape(
        drive.shape[0], count_of_groups, count_of_channels
    )
    push_real = jnp.einsum("sgc,gpc->sgp", float_values, bbar_real)
    push_imag = jnp.einsum("sgc,gpc->sgp", float_values, bbar_imag)
    next_state_real = abar_real * real_state - abar_imag * imag_state + push_real
    next_state_imaginary = abar_real * imag_state + abar_imag * real_state + push_imag
    readout_matrix = (
        jnp.einsum("jdr,dyr->jdy", next_state_real, readout_real)
        - jnp.einsum("jdr,dyr->jdy", next_state_imaginary, readout_imaginary)
        + passthrough_scale.reshape(count_of_groups, count_of_channels) * float_values
    )
    mixer = jax.nn.gelu(
        readout_matrix.reshape(drive.shape[0], count_of_groups * count_of_channels)
    ).astype(jnp.bfloat16)
    return (mixer, next_state_real, next_state_imaginary)


def slot_table(routes, expert_count, capacity):
    flat = routes.reshape(-1)
    onehot = (flat[:, None] == jnp.arange(expert_count, dtype=jnp.int32)[None, :]).astype(jnp.int32)
    before = jnp.cumsum(onehot, axis=0) - onehot
    slot = jnp.sum(before * onehot, axis=1)
    target = flat * capacity + slot
    return (
        target[None, :] == jnp.arange(expert_count * capacity, dtype=jnp.int32)[:, None]
    ).astype(jnp.bfloat16)


def body(
    tokens,
    gain_mix,
    w_in,
    decay_rate,
    frequency,
    log_step,
    input_real,
    input_imag,
    readout_real,
    readout_imaginary,
    passthrough_scale,
    state_real,
    state_imag,
    w_out,
    gain_ffn,
    expert_choice,
    expert_weight,
    w_gate,
    w_up,
    w_down,
):
    tp_count = lax.axis_size("tp")
    expert_count = lax.axis_size("ep")
    tp_rank = lax.axis_index("tp")
    row_count, local_width = tokens.shape
    full_width = local_width * tp_count
    feature_start = tp_rank * local_width
    whole = gathered_copies(tokens, "tp", 1)
    normed = rms_norm(whole, gain_mix)
    drive = jnp.dot(normed, w_in, preferred_element_type=jnp.float32).astype(jnp.bfloat16)
    mixer, next_state_real, next_state_imaginary = state_step(
        drive,
        state_real,
        state_imag,
        decay_rate,
        frequency,
        log_step,
        input_real,
        input_imag,
        readout_real,
        readout_imaginary,
        passthrough_scale,
    )
    own_columns = lax.dynamic_slice_in_dim(w_out, feature_start, local_width, 1)
    mixed = jnp.dot(
        gathered_copies(mixer, "tp", 1), own_columns, preferred_element_type=jnp.float32
    ).astype(jnp.bfloat16)
    after_mix = (tokens.astype(jnp.float32) + mixed.astype(jnp.float32)).astype(jnp.bfloat16)
    after_floats = after_mix.astype(jnp.float32)
    ffn_totals = over_copies(jnp.sum(after_floats * after_floats, axis=1), "tp")
    ffn_scale = lax.rsqrt(ffn_totals / full_width + 1e-06)
    ffn_gain_local = lax.dynamic_slice_in_dim(gain_ffn, feature_start, local_width)
    normed_ffn = (after_floats * ffn_scale[:, None] * ffn_gain_local).astype(jnp.bfloat16)
    top_count = expert_choice.shape[1]
    capacity = 2 * row_count * top_count // expert_count
    table = slot_table(expert_choice, expert_count, capacity)
    repeated = jnp.repeat(normed_ffn, top_count, axis=0)
    sent = jnp.dot(table, repeated, preferred_element_type=jnp.float32).astype(jnp.bfloat16)
    sent = sent.reshape(expert_count, capacity, local_width)
    gate_weight = w_gate[0]
    up_weight = w_up[0]
    down_weight = w_down[0]
    arrived = lax.all_to_all(sent, "ep", split_axis=0, concat_axis=0, tiled=True)
    sources, slots, _ = arrived.shape
    flat = arrived.reshape(sources * slots, local_width)
    piece = gathered_copies(flat, "tp", 1)
    gate = jnp.dot(piece, gate_weight, preferred_element_type=jnp.float32)
    upper = jnp.dot(piece, up_weight, preferred_element_type=jnp.float32)
    hidden = (jax.nn.silu(gate) * upper).astype(jnp.bfloat16)
    partial_value = jnp.dot(hidden, down_weight, preferred_element_type=jnp.float32)
    summed = summed_on_arrival(partial_value.astype(jnp.bfloat16), "tp", 1)
    results = summed.astype(jnp.bfloat16).reshape(sources, slots, local_width)
    returned = lax.all_to_all(results, "ep", split_axis=0, concat_axis=0, tiled=True)
    returned = returned.reshape(expert_count * capacity, local_width)
    picked = jnp.dot(table.T, returned, preferred_element_type=jnp.float32)
    picked = picked.reshape(row_count, top_count, local_width)
    weighted = jnp.sum(picked * expert_weight[..., None], axis=1)
    layer_out = (after_floats + weighted).astype(jnp.bfloat16)
    return (layer_out, next_state_real, next_state_imaginary)


def solution(mesh):
    return jax.shard_map(
        body,
        mesh=mesh,
        in_specs=(
            P("ep", "tp"),
            P(),
            P(None, "tp"),
            P("tp", None),
            P("tp", None),
            P("tp"),
            P("tp", None, None),
            P("tp", None, None),
            P("tp", None, None),
            P("tp", None, None),
            P("tp"),
            P("ep", "tp", None),
            P("ep", "tp", None),
            P(),
            P(),
            P("ep", None),
            P("ep", None),
            P("ep", None, "tp"),
            P("ep", None, "tp"),
            P("ep", "tp", None),
        ),
        out_specs=(P("ep", "tp"), P("ep", "tp", None), P("ep", "tp", None)),
        check_vma=False,
    )
```

profile of v0, /device:TPU:1, one launch (start us, length us, event | category | flops | bytes accessed | tf_op | source)
XLA Modules:
  0.0 180.2 jit_solution(14879596128483850)
XLA Ops:
  0.6 0.9 broadcast_in_dim.10
  1.6 1.1 reshape.114
  2.7 10.6 %all-to-all-start = ((bf16[32,2,2048]{2,1,0:T(2,128)(2,1)}), bf16[32,2,2048]{2,1,0:T(2,128)(2,1)S(1)}, u32[]{:S(2)}, u32[]{:S(2)}) async-start(bf16[32,2,2048]{2,1,0:T(2,128)(2,1)} %reshape.114), calls=%async_computation | async-start | bytes 524288 | tf_op jit(solution)/shard_map/all_to_all | solution.py:9
  13.3 0.8 copy.126
  15.6 0.8 copy.134
  16.5 0.9 copy.127
  17.4 0.9 copy.128
  18.3 0.8 add_divide_fusion
  19.1 4.6 %all-to-all-done = bf16[32,2,2048]{2,1,0:T(2,128)(2,1)S(1)} async-done(((bf16[32,2,2048]{2,1,0:T(2,128)(2,1)}), bf16[32,2,2048]{2,1,0:T(2,128)(2,1)S(1)}, u32[]{:S(2)}, u32[]{:S(2)}) %all-to-all-start) | async-done | bytes 262176 | tf_op jit(solution)/shard_map/all_to_all | solution.py:9
  26.5 0.8 reshape.116
  27.3 4.6 %all-to-all-start.1 = ((bf16[32,2,1024]{2,1,0:T(2,128)(2,1)}), bf16[32,2,1024]{2,1,0:T(2,128)(2,1)S(1)}, u32[]{:S(2)}, u32[]{:S(2)}) async-start(bf16[32,2,1024]{2,1,0:T(2,128)(2,1)} %reshape.116), calls=%async_computation.1 | async-start | bytes 262144 | tf_op jit(solution)/shard_map/all_to_all | solution.py:9
  32.4 8.9 %all-to-all-done.1 = bf16[32,2,1024]{2,1,0:T(2,128)(2,1)S(1)} async-done(((bf16[32,2,1024]{2,1,0:T(2,128)(2,1)}), bf16[32,2,1024]{2,1,0:T(2,128)(2,1)S(1)}, u32[]{:S(2)}, u32[]{:S(2)}) %all-to-all-start.1) | async-done | bytes 131104 | tf_op jit(solution)/shard_map/all_to_all | solution.py:9
  41.5 1.3 multiply_reduce_fusion
  43.5 3.8 %all-to-all-start.2 = ((f32[32,1,64]{2,1,0:T(1,128)}), f32[32,1,64]{2,1,0:T(1,128)S(1)}, u32[]{:S(2)}, u32[]{:S(2)}) async-start(f32[32,1,64]{2,1,0:T(1,128)} %broadcast_in_dim.12), calls=%async_computation.2 | async-start | bytes 32768 | tf_op jit(solution)/shard_map/all_to_all | solution.py:9
  48.1 7.8 %all-to-all-done.2 = f32[32,1,64]{2,1,0:T(1,128)S(1)} async-done(((f32[32,1,64]{2,1,0:T(1,128)}), f32[32,1,64]{2,1,0:T(1,128)S(1)}, u32[]{:S(2)}, u32[]{:S(2)}) %all-to-all-start.2) | async-done | bytes 8224 | tf_op jit(solution)/shard_map/all_to_all | solution.py:9
  56.6 35.8 %all_to_all.36 = bf16[32,2,256]{2,1,0:T(2,128)(2,1)S(1)} all-to-all(bf16[32,2,256]{2,1,0:T(2,128)(2,1)S(1)} %reshape.118), channel_id=1, replica_groups=mesh['ep'=32,'tp'=32] {'ep'}, dimensions={0} | all-to-all | bytes 65536 | tf_op jit(solution)/shard_map/all_to_all | solution.py:162
  92.7 29.0 %all_to_all.37 = bf16[32,256,64]{1,2,0:T(8,128)(2,1)S(1)} all-to-all(bf16[32,256,64]{1,2,0:T(8,128)(2,1)S(1)} %broadcast_in_dim.14), channel_id=1, replica_groups=mesh['ep'=32,'tp'=32] {'tp'}, dimensions={0} | all-to-all | bytes 2097152 | tf_op jit(solution)/shard_map/all_to_all | solution.py:9
  121.7 1.2 fusion.14
  122.9 2.6 %convolution_convert_fusion = bf16[256,2048]{1,0:T(8,128)(2,1)S(1)} fusion(bf16[256,2048]{0,1:T(8,128)(2,1)S(1)} %bitcast.64, bf16[1,256,2048]{2,1,0:T(8,128)(2,1)S(1)} %copy-done, bf16[1,2048,256]{2,1,0:T(8,128)(2,1)} %param.38, f32[256,256]{1,0:T(8,128)} %fusion.14), kind=kOutput, calls=%fused_computation | convolution fusion | flops 537788416 | bytes 4456448 | tf_op jit(solution)/shard_map/dot_general | solution.py:169
  125.5 1.3 copy.140
  126.8 6.5 %all-to-all-start.5 = ((bf16[32,256,64]{1,2,0:T(8,128)(2,1)}), bf16[32,256,64]{1,2,0:T(8,128)(2,1)S(1)}, u32[]{:S(2)}, u32[]{:S(2)}) async-start(bf16[32,256,64]{1,2,0:T(8,128)(2,1)} %bitcast.20), calls=%async_computation.5 | async-start | bytes 2097152 | tf_op jit(solution)/shard_map/all_to_all | solution.py:35
  133.5 25.1 %all-to-all-done.5 = bf16[32,256,64]{1,2,0:T(8,128)(2,1)S(1)} async-done(((bf16[32,256,64]{1,2,0:T(8,128)(2,1)}), bf16[32,256,64]{1,2,0:T(8,128)(2,1)S(1)}, u32[]{:S(2)}, u32[]{:S(2)}) %all-to-all-start.5) | async-done | bytes 1048608 | tf_op jit(solution)/shard_map/all_to_all | solution.py:35
  159.6 7.2 %all-to-all-start.6 = ((bf16[32,2,256]{2,1,0:T(2,128)(2,1)}), bf16[32,2,256]{2,1,0:T(2,128)(2,1)S(1)}, u32[]{:S(2)}, u32[]{:S(2)}) async-start(bf16[32,2,256]{2,1,0:T(2,128)(2,1)} %reshape.120), calls=%async_computation.6 | async-start | bytes 65536 | tf_op jit(solution)/shard_map/all_to_all | solution.py:172
  168.2 10.8 %all-to-all-done.6 = bf16[32,2,256]{2,1,0:T(2,128)(2,1)S(1)} async-done(((bf16[32,2,256]{2,1,0:T(2,128)(2,1)}), bf16[32,2,256]{2,1,0:T(2,128)(2,1)S(1)}, u32[]{:S(2)}, u32[]{:S(2)}) %all-to-all-start.6) | async-done | bytes 32800 | tf_op jit(solution)/shard_map/all_to_all | solution.py:172
  (67 shorter events, 11.0 us)
Async XLA Ops:
  0.6 122.3 %copy-start = (bf16[1,256,2048]{2,1,0:T(8,128)(2,1)S(1)}, bf16[1,256,2048]{2,1,0:T(8,128)(2,1)}, u32[]{:S(2)}) copy-start(bf16[1,256,2048]{2,1,0:T(8,128)(2,1)} %param.39) | copy-start | bytes 3145732
  1.6 23.9 %copy-start.2 = (bf16[2048,32]{0,1:T(8,128)(2,1)S(1)}, bf16[2048,32]{0,1:T(8,128)(2,1)}, u32[]{:S(2)}) copy-start(bf16[2048,32]{0,1:T(8,128)(2,1)} %param.22) | copy-start | bytes 393220
  1.6 23.9 %copy-start.7 = (f32[2048]{0:T(1024)S(1)}, f32[2048]{0:T(1024)}, u32[]{:S(2)}) copy-start(f32[2048]{0:T(1024)} %param.21) | copy-start | bytes 24580
  2.7 23.0 %copy-start.3 = (f32[2,64,16]{1,2,0:T(8,128)S(1)}, f32[2,64,16]{1,2,0:T(8,128)}, u32[]{:S(2)}) copy-start(f32[2,64,16]{1,2,0:T(8,128)} %param.27) | copy-start | bytes 24580
  2.7 23.1 %copy-start.4 = (f32[2,64,16]{1,2,0:T(8,128)S(1)}, f32[2,64,16]{1,2,0:T(8,128)}, u32[]{:S(2)}) copy-start(f32[2,64,16]{1,2,0:T(8,128)} %param.26) | copy-start | bytes 24580
  2.7 23.5 %copy-start.6 = (f32[2,16,64]{2,1,0:T(8,128)S(1)}, f32[2,16,64]{2,1,0:T(8,128)}, u32[]{:S(2)}) copy-start(f32[2,16,64]{2,1,0:T(8,128)} %param.28) | copy-start | bytes 24580
  2.7 21.0 %all-to-all-start = ((bf16[32,2,2048]{2,1,0:T(2,128)(2,1)}), bf16[32,2,2048]{2,1,0:T(2,128)(2,1)S(1)}, u32[]{:S(2)}, u32[]{:S(2)}) async-start(bf16[32,2,2048]{2,1,0:T(2,128)(2,1)} %reshape.114), calls=%async_computation | async-start | bytes 524288 | tf_op jit(solution)/shard_map/all_to_all | solution.py:9
  13.3 13.0 %copy-start.5 = (f32[2,16,64]{2,1,0:T(8,128)S(1)}, f32[2,16,64]{2,1,0:T(8,128)}, u32[]{:S(2)}) copy-start(f32[2,16,64]{2,1,0:T(8,128)} %param.29) | copy-start | bytes 24580
  25.7 96.0 %copy-start.1 = (bf16[1,2048,256]{2,1,0:T(8,128)(2,1)S(1)}, bf16[1,2048,256]{2,1,0:T(8,128)(2,1)}, u32[]{:S(2)}) copy-start(bf16[1,2048,256]{2,1,0:T(8,128)(2,1)} %param.37) | copy-start | bytes 3145732
  27.3 14.0 %all-to-all-start.1 = ((bf16[32,2,1024]{2,1,0:T(2,128)(2,1)}), bf16[32,2,1024]{2,1,0:T(2,128)(2,1)S(1)}, u32[]{:S(2)}, u32[]{:S(2)}) async-start(bf16[32,2,1024]{2,1,0:T(2,128)(2,1)} %reshape.116), calls=%async_computation.1 | async-start | bytes 262144 | tf_op jit(solution)/shard_map/all_to_all | solution.py:9
  43.5 12.4 %all-to-all-start.2 = ((f32[32,1,64]{2,1,0:T(1,128)}), f32[32,1,64]{2,1,0:T(1,128)S(1)}, u32[]{:S(2)}, u32[]{:S(2)}) async-start(f32[32,1,64]{2,1,0:T(1,128)} %broadcast_in_dim.12), calls=%async_computation.2 | async-start | bytes 32768 | tf_op jit(solution)/shard_map/all_to_all | solution.py:9
  122.9 43.9 %copy-start.8 = (s32[64,2]{0,1:T(2,128)S(1)}, s32[64,2]{0,1:T(2,128)}, u32[]{:S(2)}) copy-start(s32[64,2]{0,1:T(2,128)} %param.35) | copy-start | bytes 1540
  125.5 53.7 %copy-start.9 = (f32[64,2]{0,1:T(2,128)S(1)}, f32[64,2]{0,1:T(2,128)}, u32[]{:S(2)}) copy-start(f32[64,2]{0,1:T(2,128)} %param.36) | copy-start | bytes 1540
  126.8 31.8 %all-to-all-start.5 = ((bf16[32,256,64]{1,2,0:T(8,128)(2,1)}), bf16[32,256,64]{1,2,0:T(8,128)(2,1)S(1)}, u32[]{:S(2)}, u32[]{:S(2)}) async-start(bf16[32,256,64]{1,2,0:T(8,128)(2,1)} %bitcast.20), calls=%async_computation.5 | async-start | bytes 2097152 | tf_op jit(solution)/shard_map/all_to_all | solution.py:35
  159.6 19.5 %all-to-all-start.6 = ((bf16[32,2,256]{2,1,0:T(2,128)(2,1)}), bf16[32,2,256]{2,1,0:T(2,128)(2,1)S(1)}, u32[]{:S(2)}, u32[]{:S(2)}) async-start(bf16[32,2,256]{2,1,0:T(2,128)(2,1)} %reshape.120), calls=%async_computation.6 | async-start | bytes 65536 | tf_op jit(solution)/shard_map/all_to_all | solution.py:172
where the time goes:
time: 181 us; the launch traced here: 180 us
  blocking collectives  64.9 us (36%)
  waiting for transfers between devices  57.2 us (32%)
  starting transfers between devices  32.7 us (18%)
  local copies, waits for them, and re-layouts  16.1 us (9%)
  matrix products  6.41 us (4%)
  other arithmetic  1.91 us (1%)
    all_to_all x1, blocking collectives, body(): lax.all_to_all(sent, 'ep', split_axis=0, concat_axis=0, tiled=True)  35.8 us
    all_to_all x1, blocking collectives, sent_to_all(): return lax.all_to_all(copies, axis, split_axis=0, concat_axis=0, tiled=True)  29 us
    all_to_all x1, waiting for transfers between devices, summed_on_arrival(): lax.all_to_all(parts, axis, split_axis=0, concat_axis=0, tiled=True)  25.1 us
    all_to_all x3, waiting for transfers between devices, sent_to_all(): return lax.all_to_all(copies, axis, split_axis=0, concat_axis=0, tiled=True)  21.3 us
    all_to_all x3, starting transfers between devices, sent_to_all(): return lax.all_to_all(copies, axis, split_axis=0, concat_axis=0, tiled=True)  19.1 us
    all_to_all x1, waiting for transfers between devices, body(): lax.all_to_all(results, 'ep', split_axis=0, concat_axis=0, tiled=True)  10.8 us
    unnamed x36, local copies, waits for them, and re-layouts  9.19 us
    all_to_all x1, starting transfers between devices, body(): lax.all_to_all(results, 'ep', split_axis=0, concat_axis=0, tiled=True)  7.18 us
  transfers between devices with their start and end apart: 5, of which 5 were waited for; matrix products, arithmetic and copies ran while one was open for 5% of the time, Pallas kernels for 0%

commit v1 on v0

v1 whole, which is shorter than its diff:
```python
import functools

import jax
import jax.numpy as jnp
from jax import lax
from jax.experimental import pallas as pl
from jax.experimental.pallas import tpu as pltpu
from jax.sharding import Mesh
from jax.sharding import PartitionSpec as P

F32 = jnp.float32
BF16 = jnp.bfloat16
X_COUNT = 4
VMEM_LIMIT = 16 * 1024 * 1024


def exchange(parts, axis):
    return lax.all_to_all(parts, axis, split_axis=0, concat_axis=0, tiled=True)


def call(kernel, out_shape, *args, smem=(), scratch=(), flops=1_000_000):
    specs = [
        pl.BlockSpec(memory_space=pltpu.SMEM if i in smem else pltpu.VMEM) for i in range(len(args))
    ]
    outs = jax.tree.map(lambda _: pl.BlockSpec(memory_space=pltpu.VMEM), out_shape)
    return pl.pallas_call(
        kernel,
        out_shape=out_shape,
        in_specs=specs,
        out_specs=outs,
        scratch_shapes=list(scratch),
        cost_estimate=pl.CostEstimate(flops=flops, bytes_accessed=0, transcendentals=0),
        compiler_params=pltpu.CompilerParams(vmem_limit_bytes=VMEM_LIMIT),
    )(*args)


def lanes(shape):
    return lax.broadcasted_iota(jnp.int32, shape, len(shape) - 1)


def sublanes(shape):
    return lax.broadcasted_iota(jnp.int32, shape, len(shape) - 2)


def lane_roll(value, amount):
    return pltpu.roll(value, amount % value.shape[-1], value.ndim - 1)


def dot(a, b):
    return jnp.dot(a, b, preferred_element_type=F32)


def dot_nt(a, b):
    return lax.dot_general(a, b, (((1,), (1,)), ((), ())), preferred_element_type=F32)


def column_of(row):
    n = row.shape[-1]
    eye = sublanes((n, n)) == lanes((n, n))
    return jnp.sum(jnp.where(eye, jnp.broadcast_to(row, (n, n)), jnp.zeros((n, n), row.dtype)), axis=1, keepdims=True)


def spread_kernel(tokens_ref, out_ref):
    half = tokens_ref.shape[0] // 2
    values = tokens_ref[...].astype(F32)
    pair = jnp.concatenate([values[:half], values[half:]], axis=1).astype(BF16)
    for t in range(out_ref.shape[0]):
        out_ref[t] = pair


def mixer_kernel(
    arrived_ref,
    gain_ref,
    w_in_ref,
    decay_ref,
    freq_ref,
    log_step_ref,
    in_re_ref,
    in_im_ref,
    out_re_ref,
    out_im_ref,
    pass_ref,
    state_re_ref,
    state_im_ref,
    whole_ref,
    next_re_ref,
    next_im_ref,
    mixer_ref,
):
    groups, state = decay_ref.shape
    step = jnp.concatenate(
        [jnp.exp(jnp.full((1, state), log_step_ref[g], F32)) for g in range(groups)], axis=1
    )
    decay = jnp.concatenate([decay_ref[g : g + 1, :] for g in range(groups)], axis=1)
    freq = jnp.concatenate([freq_ref[g : g + 1, :] for g in range(groups)], axis=1)
    lam_re = -decay
    magnitude = jnp.exp(lam_re * step)
    abar_re = magnitude * jnp.cos(freq * step)
    abar_im = magnitude * jnp.sin(freq * step)
    denom = lam_re * lam_re + freq * freq
    numer = abar_re - 1.0
    factor_re = (numer * lam_re + abar_im * freq) / denom
    factor_im = (abar_im * lam_re - numer * freq) / denom

    def blocks(ref):
        rows = []
        for g in range(groups):
            zero = jnp.zeros_like(ref[g])
            rows.append(jnp.concatenate([ref[g] if k == g else zero for k in range(groups)], axis=1))
        return jnp.concatenate(rows, axis=0)

    in_re, in_im = blocks(in_re_ref), blocks(in_im_ref)
    bbar_re = factor_re * in_re - factor_im * in_im
    bbar_im = factor_re * in_im + factor_im * in_re

    peers, half, _ = arrived_ref.shape
    width = peers * 64
    low = lanes((half, 128)) < 64
    tops, bottoms = [], []
    for m in range(peers // 2):
        a = arrived_ref[2 * m].astype(F32)
        b = arrived_ref[2 * m + 1].astype(F32)
        tops.append(jnp.where(low, a, lane_roll(b, 64)))
        bottoms.append(jnp.where(low, lane_roll(a, 64), b))
    whole = jnp.concatenate(
        [jnp.concatenate(tops, axis=1), jnp.concatenate(bottoms, axis=1)], axis=0
    )
    whole_ref[...] = whole.astype(BF16)
    scale = lax.rsqrt(jnp.sum(whole * whole, axis=1, keepdims=True) / width + 1e-06)
    normed = (whole * scale * gain_ref[...]).astype(BF16)
    drive = dot_nt(normed, w_in_ref[...]).astype(BF16).astype(F32)

    push_re = dot(drive, bbar_re)
    push_im = dot(drive, bbar_im)
    state_re, state_im = state_re_ref[...], state_im_ref[...]
    next_re = abar_re * state_re - abar_im * state_im + push_re
    next_im = abar_re * state_im + abar_im * state_re + push_im
    next_re_ref[...] = next_re
    next_im_ref[...] = next_im
    readout = (
        dot_nt(next_re, blocks(out_re_ref))
        - dot_nt(next_im, blocks(out_im_ref))
        + pass_ref[...] * drive
    )
    mixer = jax.nn.gelu(readout)
    rows = mixer.shape[0] // 4
    packed = jnp.concatenate([mixer[q * rows : (q + 1) * rows] for q in range(4)], axis=1).astype(BF16)
    for t in range(mixer_ref.shape[0]):
        mixer_ref[t] = packed


def targets_row(choice, capacity):
    n = choice.shape[1]
    first, second = choice[0:1, :], choice[1:2, :]
    first_col, second_col = column_of(first), column_of(second)
    earlier = sublanes((n, n)) < lanes((n, n))
    one = jnp.ones((n, n), jnp.int32)
    none = jnp.zeros((n, n), jnp.int32)
    slot_a = jnp.sum(jnp.where((first_col == first) & earlier, one, none), axis=0, keepdims=True)
    slot_b = jnp.sum(
        jnp.where(first_col == second, one, none)
        + jnp.where((second_col == second) & earlier, one, none),
        axis=0,
        keepdims=True,
    )
    return first * capacity + slot_a, second * capacity + slot_b


def dispatch_kernel(
    place_ref, arrived_ref, whole_ref, w_out_ref, gain_ref, choice_ref, sent_ref, own_ref, after_ref
):
    peers, rows, _ = arrived_ref.shape
    width = whole_ref.shape[1]
    lane = lanes((rows, 128))
    quarters = []
    for q in range(4):
        tiles = []
        for m in range(peers // 4):
            tile = None
            for k in range(4):
                piece = lane_roll(arrived_ref[4 * m + k].astype(F32), (k - q) * 32)
                tile = piece if tile is None else jnp.where(lane // 32 == k, piece, tile)
            tiles.append(tile)
        quarters.append(jnp.concatenate(tiles, axis=1))
    mixer = jnp.concatenate(quarters, axis=0).astype(BF16)
    mixed = dot(mixer, w_out_ref[...]).astype(BF16).astype(F32)
    after = (whole_ref[...].astype(F32) + mixed).astype(BF16).astype(F32)
    after_ref[...] = after
    scale = lax.rsqrt(jnp.sum(after * after, axis=1, keepdims=True) / width + 1e-06)
    part = sent_ref.shape[2]
    start = pl.multiple_of(place_ref[0] * part, 128)
    gain = gain_ref[:, pl.ds(start, part)]
    normed = (after_ref[:, pl.ds(start, part)] * scale * gain).astype(BF16)
    experts, capacity, _ = sent_ref.shape
    slots = experts * capacity
    target_a, target_b = targets_row(choice_ref[...], capacity)
    slot = sublanes((slots, whole_ref.shape[0]))
    one = jnp.ones(slot.shape, F32)
    none = jnp.zeros(slot.shape, F32)
    place = jnp.where((slot == target_a) | (slot == target_b), one, none).astype(BF16)
    sent_ref[...] = dot(place, normed).astype(BF16).reshape(experts, capacity, part)
    rank = place_ref[1]
    own = after_ref[:, pl.ds(pl.multiple_of(rank // 2 * 128, 128), 128)]
    odd = jnp.broadcast_to(rank % 2, own.shape) == 1
    own_ref[...] = jnp.where(odd, lane_roll(own, 64), own)


def expert_kernel(piece_ref, gate_ref, up_ref, down_ref, parts_ref):
    count, _, part = piece_ref.shape
    gate = upper = None
    for k in range(count):
        piece = piece_ref[k]
        g = dot(piece, gate_ref[k * part : (k + 1) * part, :])
        u = dot(piece, up_ref[k * part : (k + 1) * part, :])
        gate = g if gate is None else gate + g
        upper = u if upper is None else upper + u
    hidden = (jax.nn.silu(gate) * upper).astype(BF16)
    rows = hidden.shape[0]
    low = lanes((rows, 128)) < 64
    block = 64 * count
    for m in range(part // 128):
        value = dot(hidden, down_ref[:, 2 * m * block : (2 * m + 2) * block])
        for k in range(count):
            a = value[:, k // 2 * 128 : k // 2 * 128 + 128]
            b = value[:, block + k // 2 * 128 : block + k // 2 * 128 + 128]
            if k % 2:
                joined = jnp.where(low, lane_roll(a, 64), b)
            else:
                joined = jnp.where(low, a, lane_roll(b, 64))
            parts_ref[k, :, m * 128 : (m + 1) * 128] = joined.astype(BF16)


def first_sum_kernel(arrived_ref, out_ref):
    total = arrived_ref[0].astype(F32)
    for k in range(1, arrived_ref.shape[0]):
        total = total + arrived_ref[k].astype(F32)
    turned = total.T
    for k in range(out_ref.shape[0]):
        out_ref[k] = turned[k * 64 : (k + 1) * 64, :].astype(BF16)


def slot_of(shape, axis, capacity, half):
    index = lax.broadcasted_iota(jnp.int32, shape, axis)
    short = capacity // 2
    return index // short * capacity + half * short + index % short


def second_sum_kernel(capacity, arrived_ref, out_ref):
    total = arrived_ref[0].astype(F32)
    for k in range(1, arrived_ref.shape[0]):
        total = total + arrived_ref[k].astype(F32)
    total = total.astype(BF16)
    slots = total.shape[1]
    halves = []
    for half in range(2):
        order = slot_of((slots // 2, slots), 0, capacity, half)
        one = jnp.ones(order.shape, F32)
        pick = jnp.where(order == lanes(order.shape), one, jnp.zeros_like(one)).astype(BF16)
        halves.append(dot_nt(pick, total))
    out_ref[...] = jnp.concatenate(halves, axis=1).astype(BF16).reshape(out_ref.shape)


def combine_kernel(capacity, returned_ref, choice_ref, weight_ref, own_ref, out_ref):
    returned = returned_ref[...]
    returned = returned.reshape(returned.shape[0] * returned.shape[1], 128)
    total = own_ref[:, :64]
    weight = weight_ref[...]
    for k, target in enumerate(targets_row(choice_ref[...], capacity)):
        column = column_of(target)
        picked = None
        for half in range(2):
            slot = slot_of((column.shape[0], returned.shape[0]), 1, capacity, half)
            one = jnp.ones(slot.shape, F32)
            pick = jnp.where(slot == column, one, jnp.zeros_like(one)).astype(BF16)
            value = dot(pick, returned)[:, half * 64 : half * 64 + 64]
            picked = value if picked is None else picked + value
        total = total + picked * column_of(weight[k : k + 1, :])
    out_ref[...] = total.astype(BF16)


def body(
    tokens,
    gain_mix,
    w_in,
    decay_rate,
    frequency,
    log_step,
    input_real,
    input_imag,
    readout_real,
    readout_imaginary,
    passthrough_scale,
    state_real,
    state_imag,
    w_out,
    gain_ffn,
    expert_choice,
    expert_weight,
    w_gate,
    w_up,
    w_down,
):
    x_count, y_count, experts = lax.axis_size("x"), lax.axis_size("y"), lax.axis_size("ep")
    tp_count = x_count * y_count
    rows, local_width = tokens.shape
    full_width = local_width * tp_count
    part = full_width // x_count
    capacity = 2 * rows * expert_choice.shape[1] // experts
    slots = experts * capacity
    groups, state = decay_rate.shape
    channels = passthrough_scale.shape[0]
    sds = jax.ShapeDtypeStruct

    copies = call(spread_kernel, sds((tp_count, rows // 2, 128), BF16), tokens)
    arrived = exchange(copies, ("y", "x"))
    whole, next_re, next_im, mixer = call(
        mixer_kernel,
        (
            sds((rows, full_width), BF16),
            sds((rows, groups * state), F32),
            sds((rows, groups * state), F32),
            sds((tp_count, rows // 4, 128), BF16),
        ),
        arrived,
        gain_mix.reshape(1, full_width),
        w_in.T,
        decay_rate,
        frequency,
        log_step,
        jnp.swapaxes(input_real, 1, 2),
        jnp.swapaxes(input_imag, 1, 2),
        readout_real,
        readout_imaginary,
        passthrough_scale.reshape(1, channels),
        state_real.reshape(rows, groups * state),
        state_imag.reshape(rows, groups * state),
        smem=(5,),
    )
    arrived = exchange(mixer, ("y", "x"))
    choice = expert_choice.T
    where = jnp.stack([lax.axis_index("x"), lax.axis_index(("y", "x"))]).astype(jnp.int32)
    sent, own = call(
        dispatch_kernel,
        (sds((experts, capacity, part), BF16), sds((rows, 128), F32)),
        where,
        arrived,
        whole,
        w_out,
        gain_ffn.reshape(1, full_width),
        choice,
        smem=(0,),
        scratch=(pltpu.VMEM((rows, full_width), F32),),
    )
    arrived = exchange(sent, "ep").reshape(slots, part)
    pieces = exchange(jnp.broadcast_to(arrived, (x_count, slots, part)), "x")
    parts = call(
        expert_kernel, sds((x_count, slots, part), BF16), pieces, w_gate[0], w_up[0], w_down[0]
    )
    arrived = exchange(parts, "x")
    halfway = call(first_sum_kernel, sds((y_count, local_width, slots), BF16), arrived)
    arrived = exchange(halfway, "y")
    results = call(
        functools.partial(second_sum_kernel, capacity), sds((experts, capacity // 2, 128), BF16), arrived
    )
    returned = exchange(results, "ep")
    layer_out = call(
        functools.partial(combine_kernel, capacity),
        sds((rows, local_width), BF16),
        returned,
        choice,
        expert_weight.T,
        own,
    )
    shape = state_real.shape
    return (layer_out, next_re.reshape(shape), next_im.reshape(shape))


def solution(mesh):
    tp_count = mesh.shape["tp"]
    devices = mesh.devices.reshape(mesh.shape["ep"], tp_count // X_COUNT, X_COUNT)
    tp = ("y", "x")
    return jax.shard_map(
        body,
        mesh=Mesh(devices, ("ep", "y", "x")),
        in_specs=(
            P("ep", tp),
            P(),
            P(None, tp),
            P(tp, None),
            P(tp, None),
            P(tp),
            P(tp, None, None),
            P(tp, None, None),
            P(tp, None, None),
            P(tp, None, None),
            P(tp),
            P("ep", tp, None),
            P("ep", tp, None),
            P(),
            P(),
            P("ep", None),
            P("ep", None),
            P("ep", None, tp),
            P("ep", None, tp),
            P("ep", tp, None),
        ),
        out_specs=(P("ep", tp), P("ep", tp, None), P("ep", tp, None)),
        check_vma=False,
    )
```

time: 181 us -> 166 us (0.917)
  waiting for transfers between devices: 57.2 us -> 28.4 us
  blocking collectives: 64.9 us -> 89.8 us
  starting transfers between devices: 32.7 us -> 22.7 us
  Pallas kernels: 0 us -> 7.82 us
  matrix products: 6.41 us -> 0 us
  other arithmetic: 1.91 us -> 0.08 us
    all_to_all x5 -> x3, waiting for transfers between devices: 57.2 us -> 28.4 us  [exchange(): return lax.all_to_all(parts, axis, split_axis=0, concat_axis=0, tiled=True)]
    all_to_all x2 -> x4, blocking collectives: 64.9 us -> 89.8 us  [exchange(): return lax.all_to_all(parts, axis, split_axis=0, concat_axis=0, tiled=True)]
    all_to_all x5 -> x3, starting transfers between devices: 32.7 us -> 22.7 us  [exchange(): return lax.all_to_all(parts, axis, split_axis=0, concat_axis=0, tiled=True)]
    pallas_call x0 -> x7, Pallas kernels: none -> 7.82 us  [call(): pl.pallas_call(kernel, out_shape=out_shape, in_specs=specs, out_specs=out...]
    dot_general x10 -> x0, matrix products: 6.41 us -> none  [the longest x1 2.58 us: body(): jnp.dot(hidden, down_weight, preferred_element_type=jnp.float32)]
    reshape x2 -> x4, local copies, waits for them, and re-layouts: 0.23 us -> 3.34 us  [the longest x2 1.46 us: body(): return (layer_out, next_re.reshape(shape), next_im.reshape(shape))]
    convert_element_type x5 -> x0, local copies, waits for them, and re-layouts: 2.48 us -> none  [the longest x1 1.3 us: body(): summed = summed_on_arrival(partial_value.astype(jnp.bfloat16), 'tp', 1)]
    unnamed x36 -> x38, local copies, waits for them, and re-layouts: 9.19 us -> 11.4 us
  transfers between devices with their start and end apart: 5 -> 3, of which waited for: 5 -> 3; matrix products, arithmetic and copies ran while one was open for 5% -> 2% of each run, Pallas kernels for 0% -> 0%
where the time goes in v1:
time: 166 us; the launch traced here: 164 us
  blocking collectives  89.8 us (54%)
  waiting for transfers between devices  28.4 us (17%)
  starting transfers between devices  22.7 us (14%)
  local copies, waits for them, and re-layouts  14.9 us (9%)
  Pallas kernels  7.82 us (5%)
    all_to_all x4, blocking collectives, exchange(): return lax.all_to_all(parts, axis, split_axis=0, concat_axis=0, tiled=True)  89.8 us
    all_to_all x3, waiting for transfers between devices, exchange(): return lax.all_to_all(parts, axis, split_axis=0, concat_axis=0, tiled=True)  28.4 us
    all_to_all x3, starting transfers between devices, exchange(): return lax.all_to_all(parts, axis, split_axis=0, concat_axis=0, tiled=True)  22.7 us
    unnamed x38, local copies, waits for them, and re-layouts  11.4 us
    pallas_call x7, Pallas kernels, call(): pl.pallas_call(kernel, out_shape=out_shape, in_specs=specs, out_specs=out...  7.82 us
  transfers between devices with their start and end apart: 3, of which 3 were waited for; matrix products, arithmetic and copies ran while one was open for 2% of the time, Pallas kernels for 0%

profile of v1, /device:TPU:1, one launch (start us, length us, event | category | flops | bytes accessed | tf_op | source)
XLA Modules:
  0.0 164.5 jit_solution(9355052237867768825)
XLA Ops:
  1.3 0.8 shard_map.211
  2.1 10.5 %all-to-all-start = ((bf16[32,32,128]{2,1,0:T(8,128)(2,1)}), bf16[32,32,128]{2,1,0:T(8,128)(2,1)S(1)}, u32[]{:S(2)}, u32[]{:S(2)}) async-start(bf16[32,32,128]{2,1,0:T(8,128)(2,1)} %shard_map.211), calls=%async_computation | async-start | bytes 524288 | tf_op jit(solution)/shard_map/all_to_all | solution.py:18
  12.6 0.9 reshape.32.state_re_ref
  13.6 0.9 reshape.33.state_im_ref
  14.5 8.5 %all-to-all-done.arrived_ref = bf16[32,32,128]{2,1,0:T(8,128)(2,1)S(1)} async-done(((bf16[32,32,128]{2,1,0:T(8,128)(2,1)}), bf16[32,32,128]{2,1,0:T(8,128)(2,1)S(1)}, u32[]{:S(2)}, u32[]{:S(2)}) %all-to-all-start) | async-done | bytes 262176 | tf_op jit(solution)/shard_map/all_to_all | solution.py:18
  23.0 0.9 copy-done.4
  23.9 0.7 copy-done.6
  24.7 0.7 copy-done.7
  30.2 2.0 %shard_map.212 = (bf16[64,2048]{1,0:T(8,128)(2,1)S(1)}, f32[64,128]{1,0:T(8,128)S(1)}, f32[64,128]{1,0:T(8,128)S(1)}, bf16[32,16,128]{2,1,0:T(8,128)(2,1)}) custom-call(bf16[32,32,128]{2,1,0:T(8,128)(2,1)S(1)} %all-to-all-done.arrived_ref, f32[1,2048]{1,0:T(1,128)S(1)} %bitcast.20, bf16[32,2048]{1,0:T(8,128)(2,1)S(1)} %bitcast.17, f32[2,64]{1,0:T(2,128)S(1)} %copy-done.14, ...), custom_call_target="tpu_custom_call" | custom-call | flops 1000000 | tf_op jit(solution)/shard_map/pallas_call | solution.py:26
  32.2 3.9 %all-to-all-start.1 = ((bf16[32,16,128]{2,1,0:T(8,128)(2,1)}), bf16[32,16,128]{2,1,0:T(8,128)(2,1)S(1)}, u32[]{:S(2)}, u32[]{:S(2)}) async-start(bf16[32,16,128]{2,1,0:T(8,128)(2,1)} %get-tuple-element.9), calls=%async_computation.1 | async-start | bytes 262144 | tf_op jit(solution)/shard_map/all_to_all | solution.py:18
  36.1 9.3 %all-to-all-done.1.arrived_ref = bf16[32,16,128]{2,1,0:T(8,128)(2,1)S(1)} async-done(((bf16[32,16,128]{2,1,0:T(8,128)(2,1)}), bf16[32,16,128]{2,1,0:T(8,128)(2,1)S(1)}, u32[]{:S(2)}, u32[]{:S(2)}) %all-to-all-start.1) | async-done | bytes 131104 | tf_op jit(solution)/shard_map/all_to_all | solution.py:18
  45.4 2.2 %copy-done = bf16[1024,2048]{1,0:T(8,128)(2,1)S(1)} copy-done((bf16[1024,2048]{1,0:T(8,128)(2,1)S(1)}, bf16[1024,2048]{1,0:T(8,128)(2,1)}, u32[]{:S(2)}) %copy-start) | copy-done | bytes 4194328
  49.0 1.8 %shard_map.213 = (bf16[32,8,512]{2,1,0:T(8,128)(2,1)S(1)}, f32[64,128]{1,0:T(8,128)S(1)}) custom-call(s32[2]{0:T(128)S(1)} %pad_add_fusion.place_ref, bf16[32,16,128]{2,1,0:T(8,128)(2,1)S(1)} %all-to-all-done.1.arrived_ref, bf16[64,2048]{1,0:T(8,128)(2,1)S(1)} %get-tuple-element.10.whole_ref, bf16[1024,2048]{1,0:T(8,128)(2,1)S(1)} %copy-done, ...), custom_call_target="tpu_custom_call" | custom-call | flops 1000000 | tf_op jit(solution)/shard_map/pallas_call | solution.py:26
  50.8 45.6 %all_to_all.35 = bf16[32,8,512]{2,1,0:T(8,128)(2,1)S(1)} all-to-all(bf16[32,8,512]{2,1,0:T(8,128)(2,1)S(1)} %get-tuple-element.11), channel_id=1, replica_groups=mesh['ep'=32,'y'=8,'x'=4] {'ep'}, dimensions={0} | all-to-all | bytes 524288 | tf_op jit(solution)/shard_map/all_to_all | solution.py:18
  96.5 16.6 %all_to_all.36.piece_ref = bf16[4,256,512]{2,1,0:T(8,128)(2,1)S(1)} all-to-all(bf16[4,256,512]{2,1,0:T(8,128)(2,1)S(1)} %broadcast_in_dim.3), channel_id=1, replica_groups=mesh['ep'=32,'y'=8,'x'=4] {'x'}, dimensions={0} | all-to-all | bytes 2097152 | tf_op jit(solution)/shard_map/all_to_all | solution.py:18
  113.1 1.2 shard_map.214
  114.3 15.8 %all_to_all.37.arrived_ref = bf16[4,256,512]{2,1,0:T(8,128)(2,1)S(1)} all-to-all(bf16[4,256,512]{2,1,0:T(8,128)(2,1)S(1)} %shard_map.214), channel_id=1, replica_groups=mesh['ep'=32,'y'=8,'x'=4] {'x'}, dimensions={0} | all-to-all | bytes 2097152 | tf_op jit(solution)/shard_map/all_to_all | solution.py:18
  130.3 11.8 %all_to_all.38.arrived_ref = bf16[8,64,256]{2,1,0:T(8,128)(2,1)S(1)} all-to-all(bf16[8,64,256]{2,1,0:T(8,128)(2,1)S(1)} %shard_map.215), channel_id=1, replica_groups=mesh['ep'=32,'y'=8,'x'=4] {'y'}, dimensions={0} | all-to-all | bytes 524288 | tf_op jit(solution)/shard_map/all_to_all | solution.py:18
  142.1 0.9 shard_map.216
  143.0 8.4 %all-to-all-start.6 = ((bf16[32,4,128]{2,1,0:T(4,128)(2,1)}), bf16[32,4,128]{2,1,0:T(4,128)(2,1)S(1)}, u32[]{:S(2)}, u32[]{:S(2)}) async-start(bf16[32,4,128]{2,1,0:T(4,128)(2,1)} %shard_map.216), calls=%async_computation.6 | async-start | bytes 65536 | tf_op jit(solution)/shard_map/all_to_all | solution.py:18
  151.4 0.7 reshape.36
  152.1 0.7 reshape.37
  152.8 10.6 %all-to-all-done.6.returned_ref = bf16[32,4,128]{2,1,0:T(4,128)(2,1)S(1)} async-done(((bf16[32,4,128]{2,1,0:T(4,128)(2,1)}), bf16[32,4,128]{2,1,0:T(4,128)(2,1)S(1)}, u32[]{:S(2)}, u32[]{:S(2)}) %all-to-all-start.6) | async-done | bytes 32800 | tf_op jit(solution)/shard_map/all_to_all | solution.py:18
  163.4 1.0 shard_map.217
  (37 shorter events, 7.3 us)
Async XLA Ops:
  0.6 0.7 copy-start.5
  2.1 20.9 %all-to-all-start = ((bf16[32,32,128]{2,1,0:T(8,128)(2,1)}), bf16[32,32,128]{2,1,0:T(8,128)(2,1)S(1)}, u32[]{:S(2)}, u32[]{:S(2)}) async-start(bf16[32,32,128]{2,1,0:T(8,128)(2,1)} %shard_map.211), calls=%async_computation | async-start | bytes 524288 | tf_op jit(solution)/shard_map/all_to_all | solution.py:18
  23.0 0.9 copy-start.4
  23.9 0.7 copy-start.6
  24.7 0.7 copy-start.7
  25.4 0.7 copy-start.8
  26.1 0.7 copy-start.9
  26.8 0.7 copy-start.10
  27.5 0.7 copy-start.14
  28.2 0.7 copy-start.15
  28.9 0.7 copy-start.17
  29.5 0.7 copy-start.18
  32.2 13.3 %all-to-all-start.1 = ((bf16[32,16,128]{2,1,0:T(8,128)(2,1)}), bf16[32,16,128]{2,1,0:T(8,128)(2,1)S(1)}, u32[]{:S(2)}, u32[]{:S(2)}) async-start(bf16[32,16,128]{2,1,0:T(8,128)(2,1)} %get-tuple-element.9), calls=%async_computation.1 | async-start | bytes 262144 | tf_op jit(solution)/shard_map/all_to_all | solution.py:18
  45.4 2.2 %copy-start = (bf16[1024,2048]{1,0:T(8,128)(2,1)S(1)}, bf16[1024,2048]{1,0:T(8,128)(2,1)}, u32[]{:S(2)}) copy-start(bf16[1024,2048]{1,0:T(8,128)(2,1)} %w_out_ref.1) | copy-start | bytes 12582916
  47.6 0.7 copy-start.11
  48.3 0.7 copy-start.12
  49.0 64.1 %copy-start.1 = (bf16[1,2048,256]{2,1,0:T(8,128)(2,1)S(1)}, bf16[1,2048,256]{2,1,0:T(8,128)(2,1)}, u32[]{:S(2)}) copy-start(bf16[1,2048,256]{2,1,0:T(8,128)(2,1)} %param.37) | copy-start | bytes 3145732
  49.0 64.1 %copy-start.2 = (bf16[1,2048,256]{2,1,0:T(8,128)(2,1)S(1)}, bf16[1,2048,256]{2,1,0:T(8,128)(2,1)}, u32[]{:S(2)}) copy-start(bf16[1,2048,256]{2,1,0:T(8,128)(2,1)} %param.38) | copy-start | bytes 3145732
  49.0 64.1 %copy-start.3 = (bf16[1,256,2048]{2,1,0:T(8,128)(2,1)S(1)}, bf16[1,256,2048]{2,1,0:T(8,128)(2,1)}, u32[]{:S(2)}) copy-start(bf16[1,256,2048]{2,1,0:T(8,128)(2,1)} %param.39) | copy-start | bytes 3145732
  113.1 50.3 %copy-start.13 = (s32[64,2]{0,1:T(2,128)S(1)}, s32[64,2]{0,1:T(2,128)}, u32[]{:S(2)}) copy-start(s32[64,2]{0,1:T(2,128)} %param.35) | copy-start | bytes 1540
  113.1 50.3 %copy-start.16 = (f32[64,2]{0,1:T(2,128)S(1)}, f32[64,2]{0,1:T(2,128)}, u32[]{:S(2)}) copy-start(f32[64,2]{0,1:T(2,128)} %param.36) | copy-start | bytes 1540
  143.0 20.5 %all-to-all-start.6 = ((bf16[32,4,128]{2,1,0:T(4,128)(2,1)}), bf16[32,4,128]{2,1,0:T(4,128)(2,1)S(1)}, u32[]{:S(2)}, u32[]{:S(2)}) async-start(bf16[32,4,128]{2,1,0:T(4,128)(2,1)} %shard_map.216), calls=%async_computation.6 | async-start | bytes 65536 | tf_op jit(solution)/shard_map/all_to_all | solution.py:18

commit v2 on v1

v2 whole, which is shorter than its diff:
```python
import functools

import jax
import jax.numpy as jnp
from jax import lax
from jax.experimental import pallas as pl
from jax.experimental.pallas import tpu as pltpu
from jax.sharding import Mesh
from jax.sharding import PartitionSpec as P

F32 = jnp.float32
BF16 = jnp.bfloat16
X_COUNT = 4
Y_LOW = 2
TP = ("yh", "yl", "x")
ROWS_OF_TP = ("yh", "yl")
NEAR = ("yl", "x")
FLOPS = 4_000_000_000
VMEM_LIMIT = 16 * 1024 * 1024


def exchange(parts, axis):
    return lax.all_to_all(parts, axis, split_axis=0, concat_axis=0, tiled=True)


def call(kernel, out_shape, *args, smem=(), scratch=(), flops=FLOPS):
    specs = [
        pl.BlockSpec(
            memory_space=pltpu.SMEM if i in smem else pltpu.VMEM
        )
        for i in range(len(args))
    ]
    outs = jax.tree.map(lambda _: pl.BlockSpec(memory_space=pltpu.VMEM), out_shape)
    return pl.pallas_call(
        kernel,
        out_shape=out_shape,
        in_specs=specs,
        out_specs=outs,
        scratch_shapes=list(scratch),
        cost_estimate=pl.CostEstimate(flops=flops, bytes_accessed=0, transcendentals=0),
        compiler_params=pltpu.CompilerParams(vmem_limit_bytes=VMEM_LIMIT),
    )(*args)


def lanes(shape):
    return lax.broadcasted_iota(jnp.int32, shape, len(shape) - 1)


def sublanes(shape):
    return lax.broadcasted_iota(jnp.int32, shape, len(shape) - 2)


def lane_roll(value, amount):
    return pltpu.roll(value, amount % value.shape[-1], value.ndim - 1)


def dot(a, b):
    return jnp.dot(a, b, preferred_element_type=F32)


def dot_nt(a, b):
    return lax.dot_general(a, b, (((1,), (1,)), ((), ())), preferred_element_type=F32)


def column_of(row):
    n = row.shape[-1]
    eye = sublanes((n, n)) == lanes((n, n))
    return jnp.sum(jnp.where(eye, jnp.broadcast_to(row, (n, n)), jnp.zeros((n, n), row.dtype)), axis=1, keepdims=True)


def spread_kernel(tokens_ref, out_ref):
    half = tokens_ref.shape[0] // 2
    values = tokens_ref[...].astype(F32)
    pair = jnp.concatenate([values[:half], values[half:]], axis=1).astype(BF16)
    for t in range(out_ref.shape[0]):
        out_ref[t] = pair


def targets_row(choice, capacity):
    n = choice.shape[1]
    first, second = choice[0:1, :], choice[1:2, :]
    first_col, second_col = column_of(first), column_of(second)
    earlier = sublanes((n, n)) < lanes((n, n))
    one = jnp.ones((n, n), jnp.int32)
    none = jnp.zeros((n, n), jnp.int32)
    slot_a = jnp.sum(jnp.where((first_col == first) & earlier, one, none), axis=0, keepdims=True)
    slot_b = jnp.sum(
        jnp.where(first_col == second, one, none)
        + jnp.where((second_col == second) & earlier, one, none),
        axis=0,
        keepdims=True,
    )
    return first * capacity + slot_a, second * capacity + slot_b


def slot_of(shape, axis, capacity, half):
    index = lax.broadcasted_iota(jnp.int32, shape, axis)
    short = capacity // 2
    return index // short * capacity + half * short + index % short


def prepare_kernel(
    capacity,
    decay_ref,
    freq_ref,
    log_step_ref,
    in_re_ref,
    in_im_ref,
    out_re_ref,
    out_im_ref,
    choice_ref,
    weight_ref,
    factors_ref,
    bbar_ref,
    readout_ref,
    place_ref,
    pick_ref,
    weight_out_ref,
):
    groups, state = decay_ref.shape
    step = jnp.concatenate(
        [jnp.exp(jnp.full((1, state), log_step_ref[g], F32)) for g in range(groups)], axis=1
    )
    decay = jnp.concatenate([decay_ref[g : g + 1, :] for g in range(groups)], axis=1)
    freq = jnp.concatenate([freq_ref[g : g + 1, :] for g in range(groups)], axis=1)
    lam_re = -decay
    magnitude = jnp.exp(lam_re * step)
    abar_re = magnitude * jnp.cos(freq * step)
    abar_im = magnitude * jnp.sin(freq * step)
    denom = lam_re * lam_re + freq * freq
    numer = abar_re - 1.0
    factor_re = (numer * lam_re + abar_im * freq) / denom
    factor_im = (abar_im * lam_re - numer * freq) / denom
    factors_ref[0] = jnp.broadcast_to(abar_re, factors_ref.shape[1:])
    factors_ref[1] = jnp.broadcast_to(abar_im, factors_ref.shape[1:])

    def blocks(ref):
        rows = []
        for g in range(groups):
            zero = jnp.zeros_like(ref[g])
            rows.append(jnp.concatenate([ref[g] if k == g else zero for k in range(groups)], axis=1))
        return jnp.concatenate(rows, axis=0)

    in_re, in_im = blocks(in_re_ref), blocks(in_im_ref)
    bbar_ref[0] = factor_re * in_re - factor_im * in_im
    bbar_ref[1] = factor_re * in_im + factor_im * in_re
    readout_ref[0] = blocks(out_re_ref)
    readout_ref[1] = -blocks(out_im_ref)

    target_a, target_b = targets_row(choice_ref[...], capacity)
    rows = target_a.shape[1]
    slots = place_ref.shape[0]

    def one_hot(condition):
        one = jnp.ones(condition.shape, F32)
        return jnp.where(condition, one, jnp.zeros_like(one)).astype(BF16)

    slot = sublanes((slots, rows))
    place_ref[...] = one_hot((slot == target_a) | (slot == target_b))
    weight = weight_ref[...]
    for k, target in enumerate((target_a, target_b)):
        column = column_of(target)
        for half in range(2):
            order = slot_of((rows, slots // 2), 1, capacity, half)
            pick_ref[2 * k + half] = one_hot(order == column)
        weight_out_ref[k] = jnp.broadcast_to(
            column_of(weight[k : k + 1, :]), weight_out_ref.shape[1:]
        )


def mixer_kernel(
    arrived_ref,
    gain_ref,
    w_in_ref,
    factors_ref,
    bbar_ref,
    readout_ref,
    pass_ref,
    state_re_ref,
    state_im_ref,
    whole_ref,
    next_re_ref,
    next_im_ref,
    mixer_ref,
):
    peers, half, _ = arrived_ref.shape
    width = peers * 64
    low = lanes((half, 128)) < 64
    tops, bottoms = [], []
    for m in range(peers // 2):
        a = arrived_ref[2 * m].astype(F32)
        b = arrived_ref[2 * m + 1].astype(F32)
        tops.append(jnp.where(low, a, lane_roll(b, 64)))
        bottoms.append(jnp.where(low, lane_roll(a, 64), b))
    whole = jnp.concatenate(
        [jnp.concatenate(tops, axis=1), jnp.concatenate(bottoms, axis=1)], axis=0
    )
    whole_ref[...] = whole.astype(BF16)
    scale = lax.rsqrt(jnp.sum(whole * whole, axis=1, keepdims=True) / width + 1e-06)
    normed = (whole * scale * gain_ref[...]).astype(BF16)
    drive = dot_nt(normed, w_in_ref[...]).astype(BF16).astype(F32)

    groups = state_re_ref.shape[1]
    state_re = jnp.concatenate([state_re_ref[:, g, :] for g in range(groups)], axis=1)
    state_im = jnp.concatenate([state_im_ref[:, g, :] for g in range(groups)], axis=1)
    abar_re, abar_im = factors_ref[0, 0:1, :], factors_ref[1, 0:1, :]
    next_re = abar_re * state_re - abar_im * state_im + dot(drive, bbar_ref[0])
    next_im = abar_re * state_im + abar_im * state_re + dot(drive, bbar_ref[1])
    readout = (
        dot_nt(next_re, readout_ref[0]) + dot_nt(next_im, readout_ref[1]) + pass_ref[...] * drive
    )
    mixer = jax.nn.gelu(readout)
    rows = mixer.shape[0] // 4
    packed = jnp.concatenate([mixer[q * rows : (q + 1) * rows] for q in range(4)], axis=1).astype(BF16)
    for t in range(mixer_ref.shape[0]):
        mixer_ref[t] = packed
    state = state_re_ref.shape[2]
    for g in range(groups):
        next_re_ref[:, g, :] = next_re[:, g * state : (g + 1) * state]
        next_im_ref[:, g, :] = next_im[:, g * state : (g + 1) * state]


def dispatch_kernel(
    arrived_ref, whole_ref, w_out_ref, gain_ref, place_ref, sent_ref, own_ref, after_ref
):
    peers, rows, _ = arrived_ref.shape
    width = whole_ref.shape[1]
    lane = lanes((rows, 128))
    quarters = []
    for q in range(4):
        tiles = []
        for m in range(peers // 4):
            tile = None
            for k in range(4):
                piece = lane_roll(arrived_ref[4 * m + k].astype(F32), (k - q) * 32)
                tile = piece if tile is None else jnp.where(lane // 32 == k, piece, tile)
            tiles.append(tile)
        quarters.append(jnp.concatenate(tiles, axis=1))
    mixer = jnp.concatenate(quarters, axis=0).astype(BF16)
    mixed = dot(mixer, w_out_ref[...]).astype(BF16).astype(F32)
    after = (whole_ref[...].astype(F32) + mixed).astype(BF16).astype(F32)
    after_ref[...] = after
    scale = lax.rsqrt(jnp.sum(after * after, axis=1, keepdims=True) / width + 1e-06)
    part = sent_ref.shape[2]
    rank = lax.axis_index(TP)
    start = pl.multiple_of(lax.axis_index(NEAR) * part, 128)
    gain = gain_ref[:, pl.ds(start, part)]
    normed = (after_ref[:, pl.ds(start, part)] * scale * gain).astype(BF16)
    experts, capacity, _ = sent_ref.shape
    sent_ref[...] = dot(place_ref[...], normed).astype(BF16).reshape(experts, capacity, part)
    own = after_ref[:, pl.ds(pl.multiple_of(rank // 2 * 128, 128), 128)]
    odd = jnp.broadcast_to(rank % 2, own.shape) == 1
    own_ref[...] = jnp.where(odd, lane_roll(own, 64), own)


def expert_kernel(piece_ref, gate_ref, up_ref, down_ref, parts_ref):
    pieces, _, share = piece_ref.shape
    count, _, part = parts_ref.shape
    gate = upper = None
    for k in range(pieces):
        piece = piece_ref[k]
        g = dot(piece, gate_ref[k * share : (k + 1) * share, :])
        u = dot(piece, up_ref[k * share : (k + 1) * share, :])
        gate = g if gate is None else gate + g
        upper = u if upper is None else upper + u
    hidden = (jax.nn.silu(gate) * upper).astype(BF16)
    rows = hidden.shape[0]
    low = lanes((rows, 128)) < 64
    block = 64 * count
    for m in range(part // 128):
        value = dot(hidden, down_ref[:, 2 * m * block : (2 * m + 2) * block])
        for k in range(count):
            a = value[:, k // 2 * 128 : k // 2 * 128 + 128]
            b = value[:, block + k // 2 * 128 : block + k // 2 * 128 + 128]
            if k % 2:
                joined = jnp.where(low, lane_roll(a, 64), b)
            else:
                joined = jnp.where(low, a, lane_roll(b, 64))
            parts_ref[k, :, m * 128 : (m + 1) * 128] = joined.astype(BF16)


def first_sum_kernel(arrived_ref, out_ref):
    total = arrived_ref[0].astype(F32)
    for k in range(1, arrived_ref.shape[0]):
        total = total + arrived_ref[k].astype(F32)
    turned = total.T
    for k in range(out_ref.shape[0]):
        out_ref[k] = turned[k * 64 : (k + 1) * 64, :].astype(BF16)


def second_sum_kernel(capacity, arrived_ref, out_ref):
    total = arrived_ref[0].astype(F32)
    for k in range(1, arrived_ref.shape[0]):
        total = total + arrived_ref[k].astype(F32)
    total = total.astype(BF16)
    slots = total.shape[1]
    halves = []
    for half in range(2):
        order = slot_of((slots // 2, slots), 0, capacity, half)
        one = jnp.ones(order.shape, F32)
        pick = jnp.where(order == lanes(order.shape), one, jnp.zeros_like(one)).astype(BF16)
        halves.append(dot_nt(pick, total))
    out_ref[...] = jnp.concatenate(halves, axis=1).astype(BF16).reshape(out_ref.shape)


def combine_kernel(returned_ref, pick_ref, weight_ref, own_ref, out_ref):
    returned = returned_ref[...]
    returned = returned.reshape(returned.shape[0] * returned.shape[1], 128)
    total = own_ref[:, :64]
    for k in range(2):
        picked = dot(pick_ref[2 * k], returned)[:, :64] + dot(pick_ref[2 * k + 1], returned)[:, 64:]
        total = total + picked * weight_ref[k]
    out_ref[...] = total.astype(BF16)


def body(
    tokens,
    gain_mix,
    w_in,
    decay_rate,
    frequency,
    log_step,
    input_real,
    input_imag,
    readout_real,
    readout_imaginary,
    passthrough_scale,
    state_real,
    state_imag,
    w_out,
    gain_ffn,
    expert_choice,
    expert_weight,
    w_gate,
    w_up,
    w_down,
):
    x_count, y_count, experts = lax.axis_size("x"), lax.axis_size(ROWS_OF_TP), lax.axis_size("ep")
    near = lax.axis_size(NEAR)
    tp_count = x_count * y_count
    rows, local_width = tokens.shape
    full_width = local_width * tp_count
    part = full_width // x_count
    share = full_width // near
    capacity = 2 * rows * expert_choice.shape[1] // experts
    slots = experts * capacity
    groups, state = decay_rate.shape
    channels = passthrough_scale.shape[0]
    sds = jax.ShapeDtypeStruct

    copies = call(spread_kernel, sds((tp_count, rows // 2, 128), BF16), tokens)
    arrived = exchange(copies, TP)
    factors, bbar, readout, place, picks, weights = call(
        functools.partial(prepare_kernel, capacity),
        (
            sds((2, 8, groups * state), F32),
            sds((2, channels, groups * state), F32),
            sds((2, channels, groups * state), F32),
            sds((slots, rows), BF16),
            sds((4, rows, slots // 2), BF16),
            sds((2, rows, local_width), F32),
        ),
        decay_rate,
        frequency,
        log_step,
        jnp.swapaxes(input_real, 1, 2),
        jnp.swapaxes(input_imag, 1, 2),
        readout_real,
        readout_imaginary,
        expert_choice.T,
        expert_weight.T,
        smem=(2,),
    )
    whole, next_re, next_im, mixer = call(
        mixer_kernel,
        (
            sds((rows, full_width), BF16),
            sds(state_real.shape, F32),
            sds(state_real.shape, F32),
            sds((tp_count, rows // 4, 128), BF16),
        ),
        arrived,
        gain_mix.reshape(1, full_width),
        w_in.T,
        factors,
        bbar,
        readout,
        passthrough_scale.reshape(1, channels),
        state_real,
        state_imag,
    )
    arrived = exchange(mixer, TP)
    sent, own = call(
        dispatch_kernel,
        (sds((experts, capacity, share), BF16), sds((rows, 128), F32)),
        arrived,
        whole,
        w_out,
        gain_ffn.reshape(1, full_width),
        place,
        scratch=(pltpu.VMEM((rows, full_width), F32),),
    )
    arrived = exchange(sent, "ep").reshape(slots, share)
    pieces = exchange(jnp.broadcast_to(arrived, (near, slots, share)), NEAR)
    parts = call(
        expert_kernel, sds((x_count, slots, part), BF16), pieces, w_gate[0], w_up[0], w_down[0]
    )
    arrived = exchange(parts, "x")
    halfway = call(first_sum_kernel, sds((y_count, local_width, slots), BF16), arrived)
    arrived = exchange(halfway, ROWS_OF_TP)
    results = call(
        functools.partial(second_sum_kernel, capacity), sds((experts, capacity // 2, 128), BF16), arrived
    )
    returned = exchange(results, "ep")
    layer_out = call(
        combine_kernel, sds((rows, local_width), BF16), returned, picks, weights, own
    )
    return (layer_out, next_re, next_im)


def solution(mesh):
    tp_count = mesh.shape["tp"]
    devices = mesh.devices.reshape(
        mesh.shape["ep"], tp_count // (Y_LOW * X_COUNT), Y_LOW, X_COUNT
    )
    tp = TP
    return jax.shard_map(
        body,
        mesh=Mesh(devices, ("ep", *TP)),
        in_specs=(
            P("ep", tp),
            P(),
            P(None, tp),
            P(tp, None),
            P(tp, None),
            P(tp),
            P(tp, None, None),
            P(tp, None, None),
            P(tp, None, None),
            P(tp, None, None),
            P(tp),
            P("ep", tp, None),
            P("ep", tp, None),
            P(),
            P(),
            P("ep", None),
            P("ep", None),
            P("ep", None, tp),
            P("ep", None, tp),
            P("ep", tp, None),
        ),
        out_specs=(P("ep", tp), P("ep", tp, None), P("ep", tp, None)),
        check_vma=False,
    )
```

time: 166 us -> 146 us (0.88)
  blocking collectives: 89.8 us -> 117 us
  waiting for transfers between devices: 28.4 us -> 9.41 us
  local copies, waits for them, and re-layouts: 14.9 us -> 0.87 us
  starting transfers between devices: 22.7 us -> 10.5 us
    all_to_all x4 -> x6, blocking collectives: 89.8 us -> 117 us  [exchange(): return lax.all_to_all(parts, axis, split_axis=0, concat_axis=0, tiled=True)]
    all_to_all x3 -> x1, waiting for transfers between devices: 28.4 us -> 9.41 us  [exchange(): return lax.all_to_all(parts, axis, split_axis=0, concat_axis=0, tiled=True)]
    all_to_all x3 -> x1, starting transfers between devices: 22.7 us -> 10.5 us  [exchange(): return lax.all_to_all(parts, axis, split_axis=0, concat_axis=0, tiled=True)]
    unnamed x38 -> x40, local copies, waits for them, and re-layouts: 11.4 us -> 0.8 us
    reshape x4 -> x0, local copies, waits for them, and re-layouts: 3.34 us -> none  [the longest x2 1.46 us: body(): return (layer_out, next_re.reshape(shape), next_im.reshape(shape))]
    pallas_call x7 -> x8, Pallas kernels: 7.82 us -> 6.68 us  [call(): pl.pallas_call(kernel, out_shape=out_shape, in_specs=specs, out_specs=out...]
  transfers between devices with their start and end apart: 3 -> 1, of which waited for: 3 -> 1; matrix products, arithmetic and copies ran while one was open for 2% -> 0% of each run, Pallas kernels for 0% -> 1%
where the time goes in v2:
time: 146 us; the launch traced here: 145 us
  blocking collectives  117 us (80%)
  starting transfers between devices  10.5 us (7%)
  waiting for transfers between devices  9.41 us (6%)
  Pallas kernels  6.68 us (5%)
    all_to_all x6, blocking collectives, exchange(): return lax.all_to_all(parts, axis, split_axis=0, concat_axis=0, tiled=True)  117 us
    all_to_all x1, starting transfers between devices, exchange(): return lax.all_to_all(parts, axis, split_axis=0, concat_axis=0, tiled=True)  10.5 us
    all_to_all x1, waiting for transfers between devices, exchange(): return lax.all_to_all(parts, axis, split_axis=0, concat_axis=0, tiled=True)  9.41 us
    pallas_call x8, Pallas kernels, call(): pl.pallas_call(kernel, out_shape=out_shape, in_specs=specs, out_specs=out...  6.68 us
  transfers between devices with their start and end apart: 1, of which 1 were waited for; matrix products, arithmetic and copies ran while one was open for 0% of the time, Pallas kernels for 1%

profile of v2, /device:TPU:1, one launch (start us, length us, event | category | flops | bytes accessed | tf_op | source)
XLA Modules:
  0.0 145.4 jit_solution(14791397550667905779)
XLA Ops:
  0.6 0.7 copy-done.7
  1.4 0.8 shard_map.211
  2.2 10.5 %all-to-all-start = ((bf16[32,32,128]{2,1,0:T(8,128)(2,1)}), bf16[32,32,128]{2,1,0:T(8,128)(2,1)S(1)}, u32[]{:S(2)}, u32[]{:S(2)}) async-start(bf16[32,32,128]{2,1,0:T(8,128)(2,1)} %shard_map.211), calls=%async_computation | async-start | bytes 524288 | tf_op jit(solution)/shard_map/all_to_all | solution.py:23
  12.8 0.0 copy-start.4
  12.8 0.0 copy-start.5
  12.8 0.0 copy-start.6
  12.8 0.0 copy-start.12
  12.9 0.8 shard_map.212
  13.7 9.4 %all-to-all-done.arrived_ref = bf16[32,32,128]{2,1,0:T(8,128)(2,1)S(1)} async-done(((bf16[32,32,128]{2,1,0:T(8,128)(2,1)}), bf16[32,32,128]{2,1,0:T(8,128)(2,1)S(1)}, u32[]{:S(2)}, u32[]{:S(2)}) %all-to-all-start) | async-done | bytes 262176 | tf_op jit(solution)/shard_map/all_to_all | solution.py:23
  23.2 0.0 copy-start.13
  23.2 1.4 shard_map.213
  24.6 12.7 %all_to_all.35.arrived_ref = bf16[32,16,128]{2,1,0:T(8,128)(2,1)S(1)} all-to-all(bf16[32,16,128]{2,1,0:T(8,128)(2,1)S(1)} %get-tuple-element.18), channel_id=1, replica_groups=mesh['ep'=32,'yh'=4,'yl'=2,'x'=4] {'yh','yl','x'}, dimensions={0} | all-to-all | bytes 262144 | tf_op jit(solution)/shard_map/all_to_all | solution.py:23
  37.3 0.0 copy-start.3
  37.3 1.1 shard_map.214
  38.5 39.5 %all_to_all.36 = bf16[32,8,256]{2,1,0:T(8,128)(2,1)S(1)} all-to-all(bf16[32,8,256]{2,1,0:T(8,128)(2,1)S(1)} %get-tuple-element.21), channel_id=1, replica_groups=mesh['ep'=32,'yh'=4,'yl'=2,'x'=4] {'ep'}, dimensions={0} | all-to-all | bytes 262144 | tf_op jit(solution)/shard_map/all_to_all | solution.py:23
  78.0 0.1 broadcast_in_dim.3
  78.1 15.4 %all_to_all.37.piece_ref = bf16[8,256,256]{2,1,0:T(8,128)(2,1)S(1)} all-to-all(bf16[8,256,256]{2,1,0:T(8,128)(2,1)S(1)} %broadcast_in_dim.3), channel_id=1, replica_groups=mesh['ep'=32,'yh'=4,'yl'=2,'x'=4] {'yl','x'}, dimensions={0} | all-to-all | bytes 2097152 | tf_op jit(solution)/shard_map/all_to_all | solution.py:23
  93.5 1.2 shard_map.215
  94.7 14.1 %all_to_all.38.arrived_ref = bf16[4,256,512]{2,1,0:T(8,128)(2,1)S(1)} all-to-all(bf16[4,256,512]{2,1,0:T(8,128)(2,1)S(1)} %shard_map.215), channel_id=1, replica_groups=mesh['ep'=32,'yh'=4,'yl'=2,'x'=4] {'x'}, dimensions={0} | all-to-all | bytes 2097152 | tf_op jit(solution)/shard_map/all_to_all | solution.py:23
  108.8 0.2 shard_map.216
  109.0 13.9 %all_to_all.39.arrived_ref = bf16[8,64,256]{2,1,0:T(8,128)(2,1)S(1)} all-to-all(bf16[8,64,256]{2,1,0:T(8,128)(2,1)S(1)} %shard_map.216), channel_id=1, replica_groups=mesh['ep'=32,'yh'=4,'yl'=2,'x'=4] {'yh','yl'}, dimensions={0} | all-to-all | bytes 524288 | tf_op jit(solution)/shard_map/all_to_all | solution.py:23
  122.9 0.3 shard_map.217
  123.2 21.3 %all_to_all.40.returned_ref = bf16[32,4,128]{2,1,0:T(4,128)(2,1)S(1)} all-to-all(bf16[32,4,128]{2,1,0:T(4,128)(2,1)S(1)} %shard_map.217), channel_id=1, replica_groups=mesh['ep'=32,'yh'=4,'yl'=2,'x'=4] {'ep'}, dimensions={0} | all-to-all | bytes 65536 | tf_op jit(solution)/shard_map/all_to_all | solution.py:23
  144.5 0.8 shard_map.218
  (33 shorter events, 0.1 us)
Async XLA Ops:
  0.6 0.7 copy-start.7
  1.4 11.4 %copy-start.8 = (f32[2,64,16]{1,2,0:T(8,128)S(1)}, f32[2,64,16]{1,2,0:T(8,128)}, u32[]{:S(2)}) copy-start(f32[2,64,16]{1,2,0:T(8,128)} %param.26) | copy-start | bytes 24580
  1.4 11.4 %copy-start.9 = (f32[2,64,16]{1,2,0:T(8,128)S(1)}, f32[2,64,16]{1,2,0:T(8,128)}, u32[]{:S(2)}) copy-start(f32[2,64,16]{1,2,0:T(8,128)} %param.27) | copy-start | bytes 24580
  1.4 11.4 %copy-start.10 = (f32[2,16,64]{2,1,0:T(8,128)S(1)}, f32[2,16,64]{2,1,0:T(8,128)}, u32[]{:S(2)}) copy-start(f32[2,16,64]{2,1,0:T(8,128)} %out_re_ref.1) | copy-start | bytes 24580
  1.4 11.4 %copy-start.11 = (f32[2,16,64]{2,1,0:T(8,128)S(1)}, f32[2,16,64]{2,1,0:T(8,128)}, u32[]{:S(2)}) copy-start(f32[2,16,64]{2,1,0:T(8,128)} %out_im_ref.1) | copy-start | bytes 24580
  1.4 11.4 %copy-start.14 = (f32[2,64]{1,0:T(2,128)S(1)}, f32[2,64]{1,0:T(2,128)}, u32[]{:S(2)}) copy-start(f32[2,64]{1,0:T(2,128)} %decay_ref.1) | copy-start | bytes 1540
  1.4 11.4 %copy-start.15 = (f32[2,64]{1,0:T(2,128)S(1)}, f32[2,64]{1,0:T(2,128)}, u32[]{:S(2)}) copy-start(f32[2,64]{1,0:T(2,128)} %freq_ref.1) | copy-start | bytes 1540
  1.4 11.4 %copy-start.16 = (s32[64,2]{0,1:T(2,128)S(1)}, s32[64,2]{0,1:T(2,128)}, u32[]{:S(2)}) copy-start(s32[64,2]{0,1:T(2,128)} %param.35) | copy-start | bytes 1540
  1.4 11.4 %copy-start.17 = (f32[64,2]{0,1:T(2,128)S(1)}, f32[64,2]{0,1:T(2,128)}, u32[]{:S(2)}) copy-start(f32[64,2]{0,1:T(2,128)} %param.36) | copy-start | bytes 1540
  1.4 11.4 %copy-start.18 = (f32[2]{0:T(128)S(1)}, f32[2]{0:T(128)}, u32[]{:S(2)}) copy-start(f32[2]{0:T(128)} %log_step_ref.1) | copy-start | bytes 28
  2.2 20.9 %all-to-all-start = ((bf16[32,32,128]{2,1,0:T(8,128)(2,1)}), bf16[32,32,128]{2,1,0:T(8,128)(2,1)S(1)}, u32[]{:S(2)}, u32[]{:S(2)}) async-start(bf16[32,32,128]{2,1,0:T(8,128)(2,1)} %shard_map.211), calls=%async_computation | async-start | bytes 524288 | tf_op jit(solution)/shard_map/all_to_all | solution.py:23
  12.8 10.3 %copy-start.4 = (bf16[2048,32]{0,1:T(8,128)(2,1)S(1)}, bf16[2048,32]{0,1:T(8,128)(2,1)}, u32[]{:S(2)}) copy-start(bf16[2048,32]{0,1:T(8,128)(2,1)} %param.22) | copy-start | bytes 393220
  12.8 10.3 %copy-start.5 = (f32[64,2,64]{2,1,0:T(2,128)S(1)}, f32[64,2,64]{2,1,0:T(2,128)}, u32[]{:S(2)}) copy-start(f32[64,2,64]{2,1,0:T(2,128)} %state_re_ref.1) | copy-start | bytes 98308
  12.8 10.3 %copy-start.6 = (f32[64,2,64]{2,1,0:T(2,128)S(1)}, f32[64,2,64]{2,1,0:T(2,128)}, u32[]{:S(2)}) copy-start(f32[64,2,64]{2,1,0:T(2,128)} %state_im_ref.1) | copy-start | bytes 98308
  12.8 10.3 %copy-start.12 = (f32[2048]{0:T(1024)S(1)}, f32[2048]{0:T(1024)}, u32[]{:S(2)}) copy-start(f32[2048]{0:T(1024)} %param.21) | copy-start | bytes 24580
  12.9 10.3 %copy-start.19 = (f32[32]{0:T(128)S(1)}, f32[32]{0:T(128)}, u32[]{:S(2)}) copy-start(f32[32]{0:T(128)} %param.30) | copy-start | bytes 388
  23.1 14.2 %copy-start = (bf16[1024,2048]{1,0:T(8,128)(2,1)S(1)}, bf16[1024,2048]{1,0:T(8,128)(2,1)}, u32[]{:S(2)}) copy-start(bf16[1024,2048]{1,0:T(8,128)(2,1)} %w_out_ref.1) | copy-start | bytes 12582916
  23.2 14.1 %copy-start.13 = (f32[2048]{0:T(1024)S(1)}, f32[2048]{0:T(1024)}, u32[]{:S(2)}) copy-start(f32[2048]{0:T(1024)} %param.34) | copy-start | bytes 24580
  37.3 56.2 %copy-start.1 = (bf16[1,2048,256]{2,1,0:T(8,128)(2,1)S(1)}, bf16[1,2048,256]{2,1,0:T(8,128)(2,1)}, u32[]{:S(2)}) copy-start(bf16[1,2048,256]{2,1,0:T(8,128)(2,1)} %param.37) | copy-start | bytes 3145732
  37.3 56.2 %copy-start.2 = (bf16[1,2048,256]{2,1,0:T(8,128)(2,1)S(1)}, bf16[1,2048,256]{2,1,0:T(8,128)(2,1)}, u32[]{:S(2)}) copy-start(bf16[1,2048,256]{2,1,0:T(8,128)(2,1)} %param.38) | copy-start | bytes 3145732
  37.3 56.2 %copy-start.3 = (bf16[1,256,2048]{2,1,0:T(8,128)(2,1)S(1)}, bf16[1,256,2048]{2,1,0:T(8,128)(2,1)}, u32[]{:S(2)}) copy-start(bf16[1,256,2048]{2,1,0:T(8,128)(2,1)} %param.39) | copy-start | bytes 3145732

commit v3 on v2

--- a/solution.py
+++ b/solution.py
@@ -13,7 +13,6 @@
 X_COUNT = 4
 Y_LOW = 2
 TP = ("yh", "yl", "x")
-ROWS_OF_TP = ("yh", "yl")
 NEAR = ("yl", "x")
 FLOPS = 4_000_000_000
 VMEM_LIMIT = 16 * 1024 * 1024
@@ -99,8 +98,11 @@
     return index // short * capacity + half * short + index % short
 
 
-def prepare_kernel(
+def mixer_kernel(
     capacity,
+    arrived_ref,
+    gain_ref,
+    w_in_ref,
     decay_ref,
     freq_ref,
     log_step_ref,
@@ -108,11 +110,15 @@
     in_im_ref,
     out_re_ref,
     out_im_ref,
+    pass_ref,
+    state_re_ref,
+    state_im_ref,
     choice_ref,
     weight_ref,
-    factors_ref,
-    bbar_ref,
-    readout_ref,
+    whole_ref,
+    next_re_ref,
+    next_im_ref,
+    mixer_ref,
     place_ref,
     pick_ref,
     weight_out_ref,
@@ -131,8 +137,6 @@
     numer = abar_re - 1.0
     factor_re = (numer * lam_re + abar_im * freq) / denom
     factor_im = (abar_im * lam_re - numer * freq) / denom
-    factors_ref[0] = jnp.broadcast_to(abar_re, factors_ref.shape[1:])
-    factors_ref[1] = jnp.broadcast_to(abar_im, factors_ref.shape[1:])
 
     def blocks(ref):
         rows = []
@@ -142,47 +146,9 @@
         return jnp.concatenate(rows, axis=0)
 
     in_re, in_im = blocks(in_re_ref), blocks(in_im_ref)
-    bbar_ref[0] = factor_re * in_re - factor_im * in_im
-    bbar_ref[1] = factor_re * in_im + factor_im * in_re
-    readout_ref[0] = blocks(out_re_ref)
-    readout_ref[1] = -blocks(out_im_ref)
-
-    target_a, target_b = targets_row(choice_ref[...], capacity)
-    rows = target_a.shape[1]
-    slots = place_ref.shape[0]
-
-    def one_hot(condition):
-        one = jnp.ones(condition.shape, F32)
-        return jnp.where(condition, one, jnp.zeros_like(one)).astype(BF16)
-
-    slot = sublanes((slots, rows))
-    place_ref[...] = one_hot((slot == target_a) | (slot == target_b))
-    weight = weight_ref[...]
-    for k, target in enumerate((target_a, target_b)):
-        column = column_of(target)
-        for half in range(2):
-            order = slot_of((rows, slots // 2), 1, capacity, half)
-            pick_ref[2 * k + half] = one_hot(order == column)
-        weight_out_ref[k] = jnp.broadcast_to(
-            column_of(weight[k : k + 1, :]), weight_out_ref.shape[1:]
-        )
-
-
-def mixer_kernel(
-    arrived_ref,
-    gain_ref,
-    w_in_ref,
-    factors_ref,
-    bbar_ref,
-    readout_ref,
-    pass_ref,
-    state_re_ref,
-    state_im_ref,
-    whole_ref,
-    next_re_ref,
-    next_im_ref,
-    mixer_ref,
-):
+    bbar_re = factor_re * in_re - factor_im * in_im
+    bbar_im = factor_re * in_im + factor_im * in_re
+
     peers, half, _ = arrived_ref.shape
     width = peers * 64
     low = lanes((half, 128)) < 64
@@ -200,14 +166,14 @@
     normed = (whole * scale * gain_ref[...]).astype(BF16)
     drive = dot_nt(normed, w_in_ref[...]).astype(BF16).astype(F32)
 
-    groups = state_re_ref.shape[1]
     state_re = jnp.concatenate([state_re_ref[:, g, :] for g in range(groups)], axis=1)
     state_im = jnp.concatenate([state_im_ref[:, g, :] for g in range(groups)], axis=1)
-    abar_re, abar_im = factors_ref[0, 0:1, :], factors_ref[1, 0:1, :]
-    next_re = abar_re * state_re - abar_im * state_im + dot(drive, bbar_ref[0])
-    next_im = abar_re * state_im + abar_im * state_re + dot(drive, bbar_ref[1])
+    next_re = abar_re * state_re - abar_im * state_im + dot(drive, bbar_re)
+    next_im = abar_re * state_im + abar_im * state_re + dot(drive, bbar_im)
     readout = (
-        dot_nt(next_re, readout_ref[0]) + dot_nt(next_im, readout_ref[1]) + pass_ref[...] * drive
+        dot_nt(next_re, blocks(out_re_ref))
+        - dot_nt(next_im, blocks(out_im_ref))
+        + pass_ref[...] * drive
     )
     mixer = jax.nn.gelu(readout)
     rows = mixer.shape[0] // 4
@@ -218,6 +184,26 @@
     for g in range(groups):
         next_re_ref[:, g, :] = next_re[:, g * state : (g + 1) * state]
         next_im_ref[:, g, :] = next_im[:, g * state : (g + 1) * state]
+
+    target_a, target_b = targets_row(choice_ref[...], capacity)
+    tokens = target_a.shape[1]
+    slots = place_ref.shape[0]
+
+    def one_hot(condition):
+        one = jnp.ones(condition.shape, F32)
+        return jnp.where(condition, one, jnp.zeros_like(one)).astype(BF16)
+
+    slot = sublanes((slots, tokens))
+    place_ref[...] = one_hot((slot == target_a) | (slot == target_b))
+    weight = weight_ref[...]
+    for k, target in enumerate((target_a, target_b)):
+        column = column_of(target)
+        for half in range(2):
+            order = slot_of((tokens, slots // 2), 1, capacity, half)
+            pick_ref[2 * k + half] = one_hot(order == column)
+        weight_out_ref[k] = jnp.broadcast_to(
+            column_of(weight[k : k + 1, :]), weight_out_ref.shape[1:]
+        )
 
 
 def dispatch_kernel(
@@ -279,33 +265,36 @@
             parts_ref[k, :, m * 128 : (m + 1) * 128] = joined.astype(BF16)
 
 
-def first_sum_kernel(arrived_ref, out_ref):
-    total = arrived_ref[0].astype(F32)
-    for k in range(1, arrived_ref.shape[0]):
-        total = total + arrived_ref[k].astype(F32)
-    turned = total.T
-    for k in range(out_ref.shape[0]):
-        out_ref[k] = turned[k * 64 : (k + 1) * 64, :].astype(BF16)
-
-
-def second_sum_kernel(capacity, arrived_ref, out_ref):
+def sum_kernel(capacity, arrived_ref, out_ref):
     total = arrived_ref[0].astype(F32)
     for k in range(1, arrived_ref.shape[0]):
         total = total + arrived_ref[k].astype(F32)
     total = total.astype(BF16)
-    slots = total.shape[1]
+    slots = total.shape[0]
     halves = []
     for half in range(2):
         order = slot_of((slots // 2, slots), 0, capacity, half)
         one = jnp.ones(order.shape, F32)
         pick = jnp.where(order == lanes(order.shape), one, jnp.zeros_like(one)).astype(BF16)
-        halves.append(dot_nt(pick, total))
-    out_ref[...] = jnp.concatenate(halves, axis=1).astype(BF16).reshape(out_ref.shape)
+        halves.append(dot(pick, total))
+    first, second = halves
+    experts, rows, short, _ = out_ref.shape
+    low = lanes((slots // 2, 128)) < 64
+    for m in range(rows // 2):
+        a = first[:, m * 128 : (m + 1) * 128]
+        b = second[:, m * 128 : (m + 1) * 128]
+        even = jnp.where(low, a, lane_roll(b, 64)).astype(BF16)
+        odd = jnp.where(low, lane_roll(a, 64), b).astype(BF16)
+        out_ref[:, 2 * m] = even.reshape(experts, short, 128)
+        out_ref[:, 2 * m + 1] = odd.reshape(experts, short, 128)
 
 
 def combine_kernel(returned_ref, pick_ref, weight_ref, own_ref, out_ref):
-    returned = returned_ref[...]
-    returned = returned.reshape(returned.shape[0] * returned.shape[1], 128)
+    experts, rows, short, _ = returned_ref.shape
+    returned = returned_ref[:, 0].astype(F32)
+    for k in range(1, rows):
+        returned = returned + returned_ref[:, k].astype(F32)
+    returned = returned.reshape(experts * short, 128).astype(BF16)
     total = own_ref[:, :64]
     for k in range(2):
         picked = dot(pick_ref[2 * k], returned)[:, :64] + dot(pick_ref[2 * k + 1], returned)[:, 64:]
@@ -335,12 +324,10 @@
     w_up,
     w_down,
 ):
-    x_count, y_count, experts = lax.axis_size("x"), lax.axis_size(ROWS_OF_TP), lax.axis_size("ep")
-    near = lax.axis_size(NEAR)
-    tp_count = x_count * y_count
+    near, far, experts = lax.axis_size(NEAR), lax.axis_size("yh"), lax.axis_size("ep")
+    tp_count = near * far
     rows, local_width = tokens.shape
     full_width = local_width * tp_count
-    part = full_width // x_count
     share = full_width // near
     capacity = 2 * rows * expert_choice.shape[1] // experts
     slots = experts * capacity
@@ -350,16 +337,20 @@
 
     copies = call(spread_kernel, sds((tp_count, rows // 2, 128), BF16), tokens)
     arrived = exchange(copies, TP)
-    factors, bbar, readout, place, picks, weights = call(
-        functools.partial(prepare_kernel, capacity),
+    whole, next_re, next_im, mixer, place, picks, weights = call(
+        functools.partial(mixer_kernel, capacity),
         (
-            sds((2, 8, groups * state), F32),
-            sds((2, channels, groups * state), F32),
-            sds((2, channels, groups * state), F32),
+            sds((rows, full_width), BF16),
+            sds(state_real.shape, F32),
+            sds(state_real.shape, F32),
+            sds((tp_count, rows // 4, 128), BF16),
             sds((slots, rows), BF16),
             sds((4, rows, slots // 2), BF16),
             sds((2, rows, local_width), F32),
         ),
+        arrived,
+        gain_mix.reshape(1, full_width),
+        w_in.T,
         decay_rate,
         frequency,
         log_step,
@@ -367,27 +358,12 @@
         jnp.swapaxes(input_imag, 1, 2),
         readout_real,
         readout_imaginary,
-        expert_choice.T,
-        expert_weight.T,
-        smem=(2,),
-    )
-    whole, next_re, next_im, mixer = call(
-        mixer_kernel,
-        (
-            sds((rows, full_width), BF16),
-            sds(state_real.shape, F32),
-            sds(state_real.shape, F32),
-            sds((tp_count, rows // 4, 128), BF16),
-        ),
-        arrived,
-        gain_mix.reshape(1, full_width),
-        w_in.T,
-        factors,
-        bbar,
-        readout,
         passthrough_scale.reshape(1, channels),
         state_real,
         state_imag,
+        expert_choice.T,
+        expert_weight.T,
+        smem=(5,),
     )
     arrived = exchange(mixer, TP)
     sent, own = call(
@@ -403,15 +379,20 @@
     arrived = exchange(sent, "ep").reshape(slots, share)
     pieces = exchange(jnp.broadcast_to(arrived, (near, slots, share)), NEAR)
     parts = call(
-        expert_kernel, sds((x_count, slots, part), BF16), pieces, w_gate[0], w_up[0], w_down[0]
-    )
-    arrived = exchange(parts, "x")
-    halfway = call(first_sum_kernel, sds((y_count, local_width, slots), BF16), arrived)
-    arrived = exchange(halfway, ROWS_OF_TP)
+        expert_kernel,
+        sds((near, slots, far * local_width), BF16),
+        pieces,
+        w_gate[0],
+        w_up[0],
+        w_down[0],
+    )
+    arrived = exchange(parts, NEAR)
+    short = capacity // 2
     results = call(
-        functools.partial(second_sum_kernel, capacity), sds((experts, capacity // 2, 128), BF16), arrived
-    )
-    returned = exchange(results, "ep")
+        functools.partial(sum_kernel, capacity), sds((experts, far, short, 128), BF16), arrived
+    )
+    returned = exchange(results.reshape(experts * far, short, 128), ("ep", "yh"))
+    returned = returned.reshape(experts, far, short, 128)
     layer_out = call(
         combine_kernel, sds((rows, local_width), BF16), returned, picks, weights, own
     )

time: 146 us -> 144 us (0.986)
  blocking collectives: 117 us -> 136 us
  starting transfers between devices: 10.5 us -> 0 us
  waiting for transfers between devices: 9.41 us -> 0 us
    all_to_all x6, blocking collectives: 117 us -> 136 us  [exchange(): return lax.all_to_all(parts, axis, split_axis=0, concat_axis=0, tiled=True)]
    all_to_all x1 -> x0, starting transfers between devices: 10.5 us -> none  [exchange(): return lax.all_to_all(parts, axis, split_axis=0, concat_axis=0, tiled=True)]
    all_to_all x1 -> x0, waiting for transfers between devices: 9.41 us -> none  [exchange(): return lax.all_to_all(parts, axis, split_axis=0, concat_axis=0, tiled=True)]
    pallas_call x8 -> x6, Pallas kernels: 6.68 us -> 5.63 us  [call(): pl.pallas_call(kernel, out_shape=out_shape, in_specs=specs, out_specs=out...]
  transfers between devices with their start and end apart: 1 -> 0, of which waited for: 1 -> 0; matrix products, arithmetic and copies ran while one was open for 0% -> 0% of each run, Pallas kernels for 1% -> 0%
where the time goes in v3:
time: 144 us; the launch traced here: 143 us
  blocking collectives  136 us (94%)
  Pallas kernels  5.63 us (4%)
    all_to_all x6, blocking collectives, exchange(): return lax.all_to_all(parts, axis, split_axis=0, concat_axis=0, tiled=True)  136 us
    pallas_call x6, Pallas kernels, call(): pl.pallas_call(kernel, out_shape=out_shape, in_specs=specs, out_specs=out...  5.63 us

profile of v3, /device:TPU:1, one launch (start us, length us, event | category | flops | bytes accessed | tf_op | source)
XLA Modules:
  0.0 143.1 jit_solution(5674143259967228229)
XLA Ops:
  0.6 0.0 copy-start.6
  0.6 0.0 copy-start.5
  0.7 0.0 copy-start.4
  0.7 0.0 copy-start.7
  0.7 0.7 copy-done.7
  1.4 0.0 copy-start.12
  1.4 0.0 copy-start.14
  1.5 0.1 shard_map.211
  1.6 20.7 %all_to_all.30.arrived_ref = bf16[32,32,128]{2,1,0:T(8,128)(2,1)S(1)} all-to-all(bf16[32,32,128]{2,1,0:T(8,128)(2,1)S(1)} %shard_map.211), channel_id=1, replica_groups=mesh['ep'=32,'yh'=4,'yl'=2,'x'=4] {'yh','yl','x'}, dimensions={0} | all-to-all | bytes 524288 | tf_op jit(solution)/shard_map/all_to_all | solution.py:22
  22.3 0.0 copy-done.6
  22.4 0.0 copy-start
  22.4 0.0 copy-start.13
  22.4 2.0 %shard_map.212 = (bf16[64,2048]{1,0:T(8,128)(2,1)S(1)}, f32[64,2,64]{2,1,0:T(2,128)}, f32[64,2,64]{2,1,0:T(2,128)}, bf16[32,16,128]{2,1,0:T(8,128)(2,1)S(1)}, bf...) custom-call(bf16[32,32,128]{2,1,0:T(8,128)(2,1)S(1)} %all_to_all.30.arrived_ref, ...), custom_call_target="tpu_custom_call" | custom-call | flops 4000000000 | tf_op jit(solution)/shard_map/pallas_call | solution.py:33
  24.4 12.7 %all_to_all.31.arrived_ref = bf16[32,16,128]{2,1,0:T(8,128)(2,1)S(1)} all-to-all(bf16[32,16,128]{2,1,0:T(8,128)(2,1)S(1)} %get-tuple-element.12), channel_id=1, replica_groups=mesh['ep'=32,'yh'=4,'yl'=2,'x'=4] {'yh','yl','x'}, dimensions={0} | all-to-all | bytes 262144 | tf_op jit(solution)/shard_map/all_to_all | solution.py:22
  37.1 0.0 copy-start.3
  37.2 1.1 shard_map.213
  38.3 39.5 %all_to_all.32 = bf16[32,8,256]{2,1,0:T(8,128)(2,1)S(1)} all-to-all(bf16[32,8,256]{2,1,0:T(8,128)(2,1)S(1)} %get-tuple-element.15), channel_id=1, replica_groups=mesh['ep'=32,'yh'=4,'yl'=2,'x'=4] {'ep'}, dimensions={0} | all-to-all | bytes 262144 | tf_op jit(solution)/shard_map/all_to_all | solution.py:22
  77.8 0.1 broadcast_in_dim.3
  77.9 15.4 %all_to_all.33.piece_ref = bf16[8,256,256]{2,1,0:T(8,128)(2,1)S(1)} all-to-all(bf16[8,256,256]{2,1,0:T(8,128)(2,1)S(1)} %broadcast_in_dim.3), channel_id=1, replica_groups=mesh['ep'=32,'yh'=4,'yl'=2,'x'=4] {'yl','x'}, dimensions={0} | all-to-all | bytes 2097152 | tf_op jit(solution)/shard_map/all_to_all | solution.py:22
  93.3 1.2 shard_map.214
  94.5 16.9 %all_to_all.34.arrived_ref = bf16[8,256,256]{2,1,0:T(8,128)(2,1)S(1)} all-to-all(bf16[8,256,256]{2,1,0:T(8,128)(2,1)S(1)} %shard_map.214), channel_id=1, replica_groups=mesh['ep'=32,'yh'=4,'yl'=2,'x'=4] {'yl','x'}, dimensions={0} | all-to-all | bytes 2097152 | tf_op jit(solution)/shard_map/all_to_all | solution.py:22
  111.3 0.4 shard_map.215
  111.7 30.6 %all_to_all.35 = bf16[128,4,128]{2,1,0:T(4,128)(2,1)S(1)} all-to-all(bf16[128,4,128]{2,1,0:T(4,128)(2,1)S(1)} %bitcast.15), channel_id=1, replica_groups=mesh['ep'=32,'yh'=4,'yl'=2,'x'=4] {'ep','yh'}, dimensions={0} | all-to-all | bytes 262144 | tf_op jit(solution)/shard_map/all_to_all | solution.py:22
  142.3 0.9 shard_map.216
  (29 shorter events, 0.1 us)
Async XLA Ops:
  0.6 21.7 %copy-start.6 = (f32[64,2,64]{2,1,0:T(2,128)S(1)}, f32[64,2,64]{2,1,0:T(2,128)}, u32[]{:S(2)}) copy-start(f32[64,2,64]{2,1,0:T(2,128)} %state_im_ref.1) | copy-start | bytes 98308
  0.6 21.6 %copy-start.5 = (f32[64,2,64]{2,1,0:T(2,128)S(1)}, f32[64,2,64]{2,1,0:T(2,128)}, u32[]{:S(2)}) copy-start(f32[64,2,64]{2,1,0:T(2,128)} %state_re_ref.1) | copy-start | bytes 98308
  0.7 21.6 %copy-start.4 = (bf16[2048,32]{0,1:T(8,128)(2,1)S(1)}, bf16[2048,32]{0,1:T(8,128)(2,1)}, u32[]{:S(2)}) copy-start(bf16[2048,32]{0,1:T(8,128)(2,1)} %param.22) | copy-start | bytes 393220
  0.7 0.8 copy-start.7
  1.4 20.9 %copy-start.8 = (f32[2,64,16]{1,2,0:T(8,128)S(1)}, f32[2,64,16]{1,2,0:T(8,128)}, u32[]{:S(2)}) copy-start(f32[2,64,16]{1,2,0:T(8,128)} %param.26) | copy-start | bytes 24580
  1.4 20.9 %copy-start.9 = (f32[2,64,16]{1,2,0:T(8,128)S(1)}, f32[2,64,16]{1,2,0:T(8,128)}, u32[]{:S(2)}) copy-start(f32[2,64,16]{1,2,0:T(8,128)} %param.27) | copy-start | bytes 24580
  1.4 20.9 %copy-start.10 = (f32[2,16,64]{2,1,0:T(8,128)S(1)}, f32[2,16,64]{2,1,0:T(8,128)}, u32[]{:S(2)}) copy-start(f32[2,16,64]{2,1,0:T(8,128)} %out_re_ref.1) | copy-start | bytes 24580
  1.4 20.9 %copy-start.11 = (f32[2,16,64]{2,1,0:T(8,128)S(1)}, f32[2,16,64]{2,1,0:T(8,128)}, u32[]{:S(2)}) copy-start(f32[2,16,64]{2,1,0:T(8,128)} %out_im_ref.1) | copy-start | bytes 24580
  1.4 20.9 %copy-start.12 = (f32[2048]{0:T(1024)S(1)}, f32[2048]{0:T(1024)}, u32[]{:S(2)}) copy-start(f32[2048]{0:T(1024)} %param.21) | copy-start | bytes 24580
  1.4 20.9 %copy-start.14 = (f32[2,64]{1,0:T(2,128)S(1)}, f32[2,64]{1,0:T(2,128)}, u32[]{:S(2)}) copy-start(f32[2,64]{1,0:T(2,128)} %decay_ref.1) | copy-start | bytes 1540
  1.5 20.9 %copy-start.15 = (f32[2,64]{1,0:T(2,128)S(1)}, f32[2,64]{1,0:T(2,128)}, u32[]{:S(2)}) copy-start(f32[2,64]{1,0:T(2,128)} %freq_ref.1) | copy-start | bytes 1540
  1.5 20.9 %copy-start.16 = (s32[64,2]{0,1:T(2,128)S(1)}, s32[64,2]{0,1:T(2,128)}, u32[]{:S(2)}) copy-start(s32[64,2]{0,1:T(2,128)} %param.35) | copy-start | bytes 1540
  1.5 20.9 %copy-start.17 = (f32[64,2]{0,1:T(2,128)S(1)}, f32[64,2]{0,1:T(2,128)}, u32[]{:S(2)}) copy-start(f32[64,2]{0,1:T(2,128)} %param.36) | copy-start | bytes 1540
  1.5 20.9 %copy-start.18 = (f32[2]{0:T(128)S(1)}, f32[2]{0:T(128)}, u32[]{:S(2)}) copy-start(f32[2]{0:T(128)} %log_step_ref.1) | copy-start | bytes 28
  1.5 20.9 %copy-start.19 = (f32[32]{0:T(128)S(1)}, f32[32]{0:T(128)}, u32[]{:S(2)}) copy-start(f32[32]{0:T(128)} %param.30) | copy-start | bytes 388
  22.4 14.7 %copy-start = (bf16[1024,2048]{1,0:T(8,128)(2,1)S(1)}, bf16[1024,2048]{1,0:T(8,128)(2,1)}, u32[]{:S(2)}) copy-start(bf16[1024,2048]{1,0:T(8,128)(2,1)} %w_out_ref.1) | copy-start | bytes 12582916
  22.4 14.7 %copy-start.13 = (f32[2048]{0:T(1024)S(1)}, f32[2048]{0:T(1024)}, u32[]{:S(2)}) copy-start(f32[2048]{0:T(1024)} %param.34) | copy-start | bytes 24580
  37.1 56.2 %copy-start.1 = (bf16[1,2048,256]{2,1,0:T(8,128)(2,1)S(1)}, bf16[1,2048,256]{2,1,0:T(8,128)(2,1)}, u32[]{:S(2)}) copy-start(bf16[1,2048,256]{2,1,0:T(8,128)(2,1)} %param.37) | copy-start | bytes 3145732
  37.1 56.2 %copy-start.2 = (bf16[1,2048,256]{2,1,0:T(8,128)(2,1)S(1)}, bf16[1,2048,256]{2,1,0:T(8,128)(2,1)}, u32[]{:S(2)}) copy-start(bf16[1,2048,256]{2,1,0:T(8,128)(2,1)} %param.38) | copy-start | bytes 3145732
  37.1 56.2 %copy-start.3 = (bf16[1,256,2048]{2,1,0:T(8,128)(2,1)S(1)}, bf16[1,256,2048]{2,1,0:T(8,128)(2,1)}, u32[]{:S(2)}) copy-start(bf16[1,256,2048]{2,1,0:T(8,128)(2,1)} %param.39) | copy-start | bytes 3145732

commit v4 on v3

--- a/solution.py
+++ b/solution.py
@@ -22,14 +22,20 @@
     return lax.all_to_all(parts, axis, split_axis=0, concat_axis=0, tiled=True)
 
 
-def call(kernel, out_shape, *args, smem=(), scratch=(), flops=FLOPS):
+def call(kernel, out_shape, *args, smem=(), hbm_outs=(), scratch=(), flops=FLOPS):
     specs = [
         pl.BlockSpec(
             memory_space=pltpu.SMEM if i in smem else pltpu.VMEM
         )
         for i in range(len(args))
     ]
-    outs = jax.tree.map(lambda _: pl.BlockSpec(memory_space=pltpu.VMEM), out_shape)
+    if isinstance(out_shape, tuple):
+        outs = tuple(
+            pl.BlockSpec(memory_space=pltpu.HBM if i in hbm_outs else pltpu.VMEM)
+            for i in range(len(out_shape))
+        )
+    else:
+        outs = pl.BlockSpec(memory_space=pltpu.VMEM)
     return pl.pallas_call(
         kernel,
         out_shape=out_shape,
@@ -99,7 +105,6 @@
 
 
 def mixer_kernel(
-    capacity,
     arrived_ref,
     gain_ref,
     w_in_ref,
@@ -113,15 +118,10 @@
     pass_ref,
     state_re_ref,
     state_im_ref,
-    choice_ref,
-    weight_ref,
     whole_ref,
     next_re_ref,
     next_im_ref,
     mixer_ref,
-    place_ref,
-    pick_ref,
-    weight_out_ref,
 ):
     groups, state = decay_ref.shape
     step = jnp.concatenate(
@@ -185,16 +185,42 @@
         next_re_ref[:, g, :] = next_re[:, g * state : (g + 1) * state]
         next_im_ref[:, g, :] = next_im[:, g * state : (g + 1) * state]
 
+
+def dispatch_kernel(
+    arrived_ref,
+    whole_ref,
+    w_out_ref,
+    gain_ref,
+    choice_ref,
+    weight_ref,
+    state_re_ref,
+    state_im_ref,
+    sent_ref,
+    own_ref,
+    pick_ref,
+    weight_out_ref,
+    out_re_ref,
+    out_im_ref,
+    after_ref,
+    sems,
+):
+    copies = [
+        pltpu.make_async_copy(state_re_ref, out_re_ref, sems.at[0]),
+        pltpu.make_async_copy(state_im_ref, out_im_ref, sems.at[1]),
+    ]
+    for copy in copies:
+        copy.start()
+    experts, capacity, _ = sent_ref.shape
     target_a, target_b = targets_row(choice_ref[...], capacity)
     tokens = target_a.shape[1]
-    slots = place_ref.shape[0]
+    slots = experts * capacity
 
     def one_hot(condition):
         one = jnp.ones(condition.shape, F32)
         return jnp.where(condition, one, jnp.zeros_like(one)).astype(BF16)
 
     slot = sublanes((slots, tokens))
-    place_ref[...] = one_hot((slot == target_a) | (slot == target_b))
+    place = one_hot((slot == target_a) | (slot == target_b))
     weight = weight_ref[...]
     for k, target in enumerate((target_a, target_b)):
         column = column_of(target)
@@ -204,11 +230,6 @@
         weight_out_ref[k] = jnp.broadcast_to(
             column_of(weight[k : k + 1, :]), weight_out_ref.shape[1:]
         )
-
-
-def dispatch_kernel(
-    arrived_ref, whole_ref, w_out_ref, gain_ref, place_ref, sent_ref, own_ref, after_ref
-):
     peers, rows, _ = arrived_ref.shape
     width = whole_ref.shape[1]
     lane = lanes((rows, 128))
@@ -232,11 +253,12 @@
     start = pl.multiple_of(lax.axis_index(NEAR) * part, 128)
     gain = gain_ref[:, pl.ds(start, part)]
     normed = (after_ref[:, pl.ds(start, part)] * scale * gain).astype(BF16)
-    experts, capacity, _ = sent_ref.shape
-    sent_ref[...] = dot(place_ref[...], normed).astype(BF16).reshape(experts, capacity, part)
+    sent_ref[...] = dot(place, normed).astype(BF16).reshape(experts, capacity, part)
     own = after_ref[:, pl.ds(pl.multiple_of(rank // 2 * 128, 128), 128)]
     odd = jnp.broadcast_to(rank % 2, own.shape) == 1
     own_ref[...] = jnp.where(odd, lane_roll(own, 64), own)
+    for copy in copies:
+        copy.wait()
 
 
 def expert_kernel(piece_ref, gate_ref, up_ref, down_ref, parts_ref):
@@ -337,16 +359,13 @@
 
     copies = call(spread_kernel, sds((tp_count, rows // 2, 128), BF16), tokens)
     arrived = exchange(copies, TP)
-    whole, next_re, next_im, mixer, place, picks, weights = call(
-        functools.partial(mixer_kernel, capacity),
+    whole, next_re, next_im, mixer = call(
+        mixer_kernel,
         (
             sds((rows, full_width), BF16),
             sds(state_real.shape, F32),
             sds(state_real.shape, F32),
             sds((tp_count, rows // 4, 128), BF16),
-            sds((slots, rows), BF16),
-            sds((4, rows, slots // 2), BF16),
-            sds((2, rows, local_width), F32),
         ),
         arrived,
         gain_mix.reshape(1, full_width),
@@ -361,20 +380,29 @@
         passthrough_scale.reshape(1, channels),
         state_real,
         state_imag,
-        expert_choice.T,
-        expert_weight.T,
         smem=(5,),
     )
     arrived = exchange(mixer, TP)
-    sent, own = call(
+    sent, own, picks, weights, next_re, next_im = call(
         dispatch_kernel,
-        (sds((experts, capacity, share), BF16), sds((rows, 128), F32)),
+        (
+            sds((experts, capacity, share), BF16),
+            sds((rows, 128), F32),
+            sds((4, rows, slots // 2), BF16),
+            sds((2, rows, local_width), F32),
+            sds(state_real.shape, F32),
+            sds(state_real.shape, F32),
+        ),
         arrived,
         whole,
         w_out,
         gain_ffn.reshape(1, full_width),
-        place,
-        scratch=(pltpu.VMEM((rows, full_width), F32),),
+        expert_choice.T,
+        expert_weight.T,
+        next_re,
+        next_im,
+        hbm_outs=(4, 5),
+        scratch=(pltpu.VMEM((rows, full_width), F32), pltpu.SemaphoreType.DMA((2,))),
     )
     arrived = exchange(sent, "ep").reshape(slots, share)
     pieces = exchange(jnp.broadcast_to(arrived, (near, slots, share)), NEAR)

time: 144 us -> 143 us (level)
  no operation moved by 1% of the time
where the time goes in v4:
time: 143 us
  blocking collectives  136 us (95%)
  Pallas kernels  5.51 us (4%)
    all_to_all x6, blocking collectives, exchange(): return lax.all_to_all(parts, axis, split_axis=0, concat_axis=0, tiled=True)  136 us
    pallas_call x6, Pallas kernels, call(): pl.pallas_call(kernel, out_shape=out_shape, in_specs=specs, out_specs=out...  5.51 us

profile of v4, /device:TPU:1, one launch (start us, length us, event | category | flops | bytes accessed | tf_op | source)
XLA Modules:
  0.0 143.1 jit_solution(14336611253457804786)
XLA Ops:
  0.7 0.7 copy-done.7
  1.5 0.1 shard_map.211
  1.6 20.7 %all_to_all.30.arrived_ref = bf16[32,32,128]{2,1,0:T(8,128)(2,1)S(1)} all-to-all(bf16[32,32,128]{2,1,0:T(8,128)(2,1)S(1)} %shard_map.211), channel_id=1, replica_groups=mesh['ep'=32,'yh'=4,'yl'=2,'x'=4] {'yh','yl','x'}, dimensions={0} | all-to-all | bytes 524288 | tf_op jit(solution)/shard_map/all_to_all | solution.py:22
  22.3 0.0 copy-done.5
  22.4 0.0 copy-start
  22.4 0.0 copy-start.13
  22.4 0.0 copy-start.16
  22.4 0.0 copy-start.17
  22.4 1.4 shard_map.212
  23.8 12.7 %all_to_all.31.arrived_ref = bf16[32,16,128]{2,1,0:T(8,128)(2,1)S(1)} all-to-all(bf16[32,16,128]{2,1,0:T(8,128)(2,1)S(1)} %get-tuple-element.13), channel_id=1, replica_groups=mesh['ep'=32,'yh'=4,'yl'=2,'x'=4] {'yh','yl','x'}, dimensions={0} | all-to-all | bytes 262144 | tf_op jit(solution)/shard_map/all_to_all | solution.py:22
  36.5 0.0 copy-done.13
  36.5 0.0 copy-start.1
  36.5 0.0 copy-start.2
  36.5 0.0 copy-start.3
  36.5 1.7 %shard_map.213 = (bf16[32,8,256]{2,1,0:T(8,128)(2,1)S(1)}, f32[64,128]{1,0:T(8,128)S(1)}, bf16[4,64,128]{2,1,0:T(8,128)(2,1)S(1)}, f32[2,64,64]{2,1,0:T(8,128)S(...) custom-call(bf16[32,16,128]{2,1,0:T(8,128)(2,1)S(1)} %all_to_all.31.arrived_ref, ...), custom_call_target="tpu_custom_call" | custom-call | flops 4000000000 | tf_op jit(solution)/shard_map/pallas_call | solution.py:39
  38.2 39.5 %all_to_all.32 = bf16[32,8,256]{2,1,0:T(8,128)(2,1)S(1)} all-to-all(bf16[32,8,256]{2,1,0:T(8,128)(2,1)S(1)} %get-tuple-element.17), channel_id=1, replica_groups=mesh['ep'=32,'yh'=4,'yl'=2,'x'=4] {'ep'}, dimensions={0} | all-to-all | bytes 262144 | tf_op jit(solution)/shard_map/all_to_all | solution.py:22
  77.8 0.1 broadcast_in_dim.3
  77.8 15.4 %all_to_all.33.piece_ref = bf16[8,256,256]{2,1,0:T(8,128)(2,1)S(1)} all-to-all(bf16[8,256,256]{2,1,0:T(8,128)(2,1)S(1)} %broadcast_in_dim.3), channel_id=1, replica_groups=mesh['ep'=32,'yh'=4,'yl'=2,'x'=4] {'yl','x'}, dimensions={0} | all-to-all | bytes 2097152 | tf_op jit(solution)/shard_map/all_to_all | solution.py:22
  93.2 0.0 copy-done.3
  93.2 1.2 shard_map.214
  94.4 16.9 %all_to_all.34.arrived_ref = bf16[8,256,256]{2,1,0:T(8,128)(2,1)S(1)} all-to-all(bf16[8,256,256]{2,1,0:T(8,128)(2,1)S(1)} %shard_map.214), channel_id=1, replica_groups=mesh['ep'=32,'yh'=4,'yl'=2,'x'=4] {'yl','x'}, dimensions={0} | all-to-all | bytes 2097152 | tf_op jit(solution)/shard_map/all_to_all | solution.py:22
  111.3 0.4 shard_map.215
  111.6 30.6 %all_to_all.35 = bf16[128,4,128]{2,1,0:T(4,128)(2,1)S(1)} all-to-all(bf16[128,4,128]{2,1,0:T(4,128)(2,1)S(1)} %bitcast.15), channel_id=1, replica_groups=mesh['ep'=32,'yh'=4,'yl'=2,'x'=4] {'ep','yh'}, dimensions={0} | all-to-all | bytes 262144 | tf_op jit(solution)/shard_map/all_to_all | solution.py:22
  142.2 0.9 shard_map.216
  (29 shorter events, 0.1 us)
Async XLA Ops:
  0.6 21.6 %copy-start.6 = (f32[64,2,64]{2,1,0:T(2,128)S(1)}, f32[64,2,64]{2,1,0:T(2,128)}, u32[]{:S(2)}) copy-start(f32[64,2,64]{2,1,0:T(2,128)} %state_im_ref.1) | copy-start | bytes 98308
  0.6 21.6 %copy-start.5 = (f32[64,2,64]{2,1,0:T(2,128)S(1)}, f32[64,2,64]{2,1,0:T(2,128)}, u32[]{:S(2)}) copy-start(f32[64,2,64]{2,1,0:T(2,128)} %state_re_ref.1) | copy-start | bytes 98308
  0.7 21.6 %copy-start.4 = (bf16[2048,32]{0,1:T(8,128)(2,1)S(1)}, bf16[2048,32]{0,1:T(8,128)(2,1)}, u32[]{:S(2)}) copy-start(bf16[2048,32]{0,1:T(8,128)(2,1)} %param.22) | copy-start | bytes 393220
  0.7 0.8 copy-start.7
  1.4 20.9 %copy-start.8 = (f32[2,64,16]{1,2,0:T(8,128)S(1)}, f32[2,64,16]{1,2,0:T(8,128)}, u32[]{:S(2)}) copy-start(f32[2,64,16]{1,2,0:T(8,128)} %param.26) | copy-start | bytes 24580
  1.4 20.9 %copy-start.9 = (f32[2,64,16]{1,2,0:T(8,128)S(1)}, f32[2,64,16]{1,2,0:T(8,128)}, u32[]{:S(2)}) copy-start(f32[2,64,16]{1,2,0:T(8,128)} %param.27) | copy-start | bytes 24580
  1.4 20.9 %copy-start.10 = (f32[2,16,64]{2,1,0:T(8,128)S(1)}, f32[2,16,64]{2,1,0:T(8,128)}, u32[]{:S(2)}) copy-start(f32[2,16,64]{2,1,0:T(8,128)} %out_re_ref.1) | copy-start | bytes 24580
  1.4 20.9 %copy-start.11 = (f32[2,16,64]{2,1,0:T(8,128)S(1)}, f32[2,16,64]{2,1,0:T(8,128)}, u32[]{:S(2)}) copy-start(f32[2,16,64]{2,1,0:T(8,128)} %out_im_ref.1) | copy-start | bytes 24580
  1.4 20.9 %copy-start.12 = (f32[2048]{0:T(1024)S(1)}, f32[2048]{0:T(1024)}, u32[]{:S(2)}) copy-start(f32[2048]{0:T(1024)} %param.21) | copy-start | bytes 24580
  1.4 20.9 %copy-start.14 = (f32[2,64]{1,0:T(2,128)S(1)}, f32[2,64]{1,0:T(2,128)}, u32[]{:S(2)}) copy-start(f32[2,64]{1,0:T(2,128)} %decay_ref.1) | copy-start | bytes 1540
  1.5 20.9 %copy-start.15 = (f32[2,64]{1,0:T(2,128)S(1)}, f32[2,64]{1,0:T(2,128)}, u32[]{:S(2)}) copy-start(f32[2,64]{1,0:T(2,128)} %freq_ref.1) | copy-start | bytes 1540
  1.5 20.9 %copy-start.18 = (f32[2]{0:T(128)S(1)}, f32[2]{0:T(128)}, u32[]{:S(2)}) copy-start(f32[2]{0:T(128)} %log_step_ref.1) | copy-start | bytes 28
  1.5 20.9 %copy-start.19 = (f32[32]{0:T(128)S(1)}, f32[32]{0:T(128)}, u32[]{:S(2)}) copy-start(f32[32]{0:T(128)} %param.30) | copy-start | bytes 388
  22.4 14.1 %copy-start = (bf16[1024,2048]{1,0:T(8,128)(2,1)S(1)}, bf16[1024,2048]{1,0:T(8,128)(2,1)}, u32[]{:S(2)}) copy-start(bf16[1024,2048]{1,0:T(8,128)(2,1)} %w_out_ref.1) | copy-start | bytes 12582916
  22.4 14.1 %copy-start.13 = (f32[2048]{0:T(1024)S(1)}, f32[2048]{0:T(1024)}, u32[]{:S(2)}) copy-start(f32[2048]{0:T(1024)} %param.34) | copy-start | bytes 24580
  22.4 14.1 %copy-start.16 = (s32[64,2]{0,1:T(2,128)S(1)}, s32[64,2]{0,1:T(2,128)}, u32[]{:S(2)}) copy-start(s32[64,2]{0,1:T(2,128)} %param.35) | copy-start | bytes 1540
  22.4 14.1 %copy-start.17 = (f32[64,2]{0,1:T(2,128)S(1)}, f32[64,2]{0,1:T(2,128)}, u32[]{:S(2)}) copy-start(f32[64,2]{0,1:T(2,128)} %param.36) | copy-start | bytes 1540
  36.5 56.7 %copy-start.1 = (bf16[1,2048,256]{2,1,0:T(8,128)(2,1)S(1)}, bf16[1,2048,256]{2,1,0:T(8,128)(2,1)}, u32[]{:S(2)}) copy-start(bf16[1,2048,256]{2,1,0:T(8,128)(2,1)} %param.37) | copy-start | bytes 3145732
  36.5 56.7 %copy-start.2 = (bf16[1,2048,256]{2,1,0:T(8,128)(2,1)S(1)}, bf16[1,2048,256]{2,1,0:T(8,128)(2,1)}, u32[]{:S(2)}) copy-start(bf16[1,2048,256]{2,1,0:T(8,128)(2,1)} %param.38) | copy-start | bytes 3145732
  36.5 56.7 %copy-start.3 = (bf16[1,256,2048]{2,1,0:T(8,128)(2,1)S(1)}, bf16[1,256,2048]{2,1,0:T(8,128)(2,1)}, u32[]{:S(2)}) copy-start(bf16[1,256,2048]{2,1,0:T(8,128)(2,1)} %param.39) | copy-start | bytes 3145732

commit v5 on v4

--- a/solution.py
+++ b/solution.py
@@ -193,23 +193,12 @@
     gain_ref,
     choice_ref,
     weight_ref,
-    state_re_ref,
-    state_im_ref,
     sent_ref,
     own_ref,
     pick_ref,
     weight_out_ref,
-    out_re_ref,
-    out_im_ref,
     after_ref,
-    sems,
 ):
-    copies = [
-        pltpu.make_async_copy(state_re_ref, out_re_ref, sems.at[0]),
-        pltpu.make_async_copy(state_im_ref, out_im_ref, sems.at[1]),
-    ]
-    for copy in copies:
-        copy.start()
     experts, capacity, _ = sent_ref.shape
     target_a, target_b = targets_row(choice_ref[...], capacity)
     tokens = target_a.shape[1]
@@ -257,11 +246,26 @@
     own = after_ref[:, pl.ds(pl.multiple_of(rank // 2 * 128, 128), 128)]
     odd = jnp.broadcast_to(rank % 2, own.shape) == 1
     own_ref[...] = jnp.where(odd, lane_roll(own, 64), own)
+
+
+def expert_kernel(
+    piece_ref,
+    gate_ref,
+    up_ref,
+    down_ref,
+    state_re_ref,
+    state_im_ref,
+    parts_ref,
+    out_re_ref,
+    out_im_ref,
+    sems,
+):
+    copies = [
+        pltpu.make_async_copy(state_re_ref, out_re_ref, sems.at[0]),
+        pltpu.make_async_copy(state_im_ref, out_im_ref, sems.at[1]),
+    ]
     for copy in copies:
-        copy.wait()
-
-
-def expert_kernel(piece_ref, gate_ref, up_ref, down_ref, parts_ref):
+        copy.start()
     pieces, _, share = piece_ref.shape
     count, _, part = parts_ref.shape
     gate = upper = None
@@ -285,6 +289,8 @@
             else:
                 joined = jnp.where(low, a, lane_roll(b, 64))
             parts_ref[k, :, m * 128 : (m + 1) * 128] = joined.astype(BF16)
+    for copy in copies:
+        copy.wait()
 
 
 def sum_kernel(capacity, arrived_ref, out_ref):
@@ -383,15 +389,13 @@
         smem=(5,),
     )
     arrived = exchange(mixer, TP)
-    sent, own, picks, weights, next_re, next_im = call(
+    sent, own, picks, weights = call(
         dispatch_kernel,
         (
             sds((experts, capacity, share), BF16),
             sds((rows, 128), F32),
             sds((4, rows, slots // 2), BF16),
             sds((2, rows, local_width), F32),
-            sds(state_real.shape, F32),
-            sds(state_real.shape, F32),
         ),
         arrived,
         whole,
@@ -399,20 +403,25 @@
         gain_ffn.reshape(1, full_width),
         expert_choice.T,
         expert_weight.T,
-        next_re,
-        next_im,
-        hbm_outs=(4, 5),
-        scratch=(pltpu.VMEM((rows, full_width), F32), pltpu.SemaphoreType.DMA((2,))),
+        scratch=(pltpu.VMEM((rows, full_width), F32),),
     )
     arrived = exchange(sent, "ep").reshape(slots, share)
     pieces = exchange(jnp.broadcast_to(arrived, (near, slots, share)), NEAR)
-    parts = call(
+    parts, next_re, next_im = call(
         expert_kernel,
-        sds((near, slots, far * local_width), BF16),
+        (
+            sds((near, slots, far * local_width), BF16),
+            sds(state_real.shape, F32),
+            sds(state_real.shape, F32),
+        ),
         pieces,
         w_gate[0],
         w_up[0],
         w_down[0],
+        next_re,
+        next_im,
+        hbm_outs=(1, 2),
+        scratch=(pltpu.SemaphoreType.DMA((2,)),),
     )
     arrived = exchange(parts, NEAR)
     short = capacity // 2

time: 143 us -> 143 us (level)
  no operation moved by 1% of the time
where the time goes in v5:
time: 143 us
  blocking collectives  136 us (95%)
  Pallas kernels  5.01 us (4%)
    all_to_all x6, blocking collectives, exchange(): return lax.all_to_all(parts, axis, split_axis=0, concat_axis=0, tiled=True)  136 us
    pallas_call x6, Pallas kernels, call(): pl.pallas_call(kernel, out_shape=out_shape, in_specs=specs, out_specs=out...  5.01 us

profile of v5, /device:TPU:1, one launch (start us, length us, event | category | flops | bytes accessed | tf_op | source)
XLA Modules:
  0.0 142.6 jit_solution(10064219652095245181)
XLA Ops:
  0.6 0.0 copy-start.6
  0.7 0.7 copy-done.7
  1.5 0.1 shard_map.211
  1.6 20.7 %all_to_all.30.arrived_ref = bf16[32,32,128]{2,1,0:T(8,128)(2,1)S(1)} all-to-all(bf16[32,32,128]{2,1,0:T(8,128)(2,1)S(1)} %shard_map.211), channel_id=1, replica_groups=mesh['ep'=32,'yh'=4,'yl'=2,'x'=4] {'yh','yl','x'}, dimensions={0} | all-to-all | bytes 524288 | tf_op jit(solution)/shard_map/all_to_all | solution.py:22
  22.3 0.0 copy-done.5
  22.4 0.0 copy-start
  22.4 0.0 copy-start.13
  22.4 0.0 copy-start.16
  22.4 0.0 copy-start.17
  22.4 1.4 shard_map.212
  23.8 12.7 %all_to_all.31.arrived_ref = bf16[32,16,128]{2,1,0:T(8,128)(2,1)S(1)} all-to-all(bf16[32,16,128]{2,1,0:T(8,128)(2,1)S(1)} %get-tuple-element.14), channel_id=1, replica_groups=mesh['ep'=32,'yh'=4,'yl'=2,'x'=4] {'yh','yl','x'}, dimensions={0} | all-to-all | bytes 262144 | tf_op jit(solution)/shard_map/all_to_all | solution.py:22
  36.5 0.0 copy-done.13
  36.5 0.0 copy-start.1
  36.5 0.0 copy-start.2
  36.5 0.0 copy-start.3
  36.5 1.1 shard_map.213
  37.7 39.5 %all_to_all.32 = bf16[32,8,256]{2,1,0:T(8,128)(2,1)S(1)} all-to-all(bf16[32,8,256]{2,1,0:T(8,128)(2,1)S(1)} %get-tuple-element.16), channel_id=1, replica_groups=mesh['ep'=32,'yh'=4,'yl'=2,'x'=4] {'ep'}, dimensions={0} | all-to-all | bytes 262144 | tf_op jit(solution)/shard_map/all_to_all | solution.py:22
  77.2 0.1 broadcast_in_dim.3
  77.3 15.4 %all_to_all.33.piece_ref = bf16[8,256,256]{2,1,0:T(8,128)(2,1)S(1)} all-to-all(bf16[8,256,256]{2,1,0:T(8,128)(2,1)S(1)} %broadcast_in_dim.3), channel_id=1, replica_groups=mesh['ep'=32,'yh'=4,'yl'=2,'x'=4] {'yl','x'}, dimensions={0} | all-to-all | bytes 2097152 | tf_op jit(solution)/shard_map/all_to_all | solution.py:22
  92.7 1.2 shard_map.214
  93.9 16.8 %all_to_all.34.arrived_ref = bf16[8,256,256]{2,1,0:T(8,128)(2,1)S(1)} all-to-all(bf16[8,256,256]{2,1,0:T(8,128)(2,1)S(1)} %get-tuple-element.19), channel_id=1, replica_groups=mesh['ep'=32,'yh'=4,'yl'=2,'x'=4] {'yl','x'}, dimensions={0} | all-to-all | bytes 2097152 | tf_op jit(solution)/shard_map/all_to_all | solution.py:22
  110.7 0.4 shard_map.215
  111.1 30.6 %all_to_all.35 = bf16[128,4,128]{2,1,0:T(4,128)(2,1)S(1)} all-to-all(bf16[128,4,128]{2,1,0:T(4,128)(2,1)S(1)} %bitcast.15), channel_id=1, replica_groups=mesh['ep'=32,'yh'=4,'yl'=2,'x'=4] {'ep','yh'}, dimensions={0} | all-to-all | bytes 262144 | tf_op jit(solution)/shard_map/all_to_all | solution.py:22
  141.7 0.9 shard_map.216
  (29 shorter events, 0.1 us)
Async XLA Ops:
  0.6 21.6 %copy-start.6 = (f32[64,2,64]{2,1,0:T(2,128)S(1)}, f32[64,2,64]{2,1,0:T(2,128)}, u32[]{:S(2)}) copy-start(f32[64,2,64]{2,1,0:T(2,128)} %state_im_ref.1) | copy-start | bytes 98308
  0.6 21.6 %copy-start.5 = (f32[64,2,64]{2,1,0:T(2,128)S(1)}, f32[64,2,64]{2,1,0:T(2,128)}, u32[]{:S(2)}) copy-start(f32[64,2,64]{2,1,0:T(2,128)} %state_re_ref.1) | copy-start | bytes 98308
  0.7 21.6 %copy-start.4 = (bf16[2048,32]{0,1:T(8,128)(2,1)S(1)}, bf16[2048,32]{0,1:T(8,128)(2,1)}, u32[]{:S(2)}) copy-start(bf16[2048,32]{0,1:T(8,128)(2,1)} %param.22) | copy-start | bytes 393220
  0.7 0.8 copy-start.7
  1.4 20.9 %copy-start.8 = (f32[2,64,16]{1,2,0:T(8,128)S(1)}, f32[2,64,16]{1,2,0:T(8,128)}, u32[]{:S(2)}) copy-start(f32[2,64,16]{1,2,0:T(8,128)} %param.26) | copy-start | bytes 24580
  1.4 20.9 %copy-start.9 = (f32[2,64,16]{1,2,0:T(8,128)S(1)}, f32[2,64,16]{1,2,0:T(8,128)}, u32[]{:S(2)}) copy-start(f32[2,64,16]{1,2,0:T(8,128)} %param.27) | copy-start | bytes 24580
  1.4 20.9 %copy-start.10 = (f32[2,16,64]{2,1,0:T(8,128)S(1)}, f32[2,16,64]{2,1,0:T(8,128)}, u32[]{:S(2)}) copy-start(f32[2,16,64]{2,1,0:T(8,128)} %out_re_ref.1) | copy-start | bytes 24580
  1.4 20.9 %copy-start.11 = (f32[2,16,64]{2,1,0:T(8,128)S(1)}, f32[2,16,64]{2,1,0:T(8,128)}, u32[]{:S(2)}) copy-start(f32[2,16,64]{2,1,0:T(8,128)} %out_im_ref.1) | copy-start | bytes 24580
  1.4 20.9 %copy-start.12 = (f32[2048]{0:T(1024)S(1)}, f32[2048]{0:T(1024)}, u32[]{:S(2)}) copy-start(f32[2048]{0:T(1024)} %param.21) | copy-start | bytes 24580
  1.4 20.9 %copy-start.14 = (f32[2,64]{1,0:T(2,128)S(1)}, f32[2,64]{1,0:T(2,128)}, u32[]{:S(2)}) copy-start(f32[2,64]{1,0:T(2,128)} %decay_ref.1) | copy-start | bytes 1540
  1.5 20.9 %copy-start.15 = (f32[2,64]{1,0:T(2,128)S(1)}, f32[2,64]{1,0:T(2,128)}, u32[]{:S(2)}) copy-start(f32[2,64]{1,0:T(2,128)} %freq_ref.1) | copy-start | bytes 1540
  1.5 20.9 %copy-start.18 = (f32[2]{0:T(128)S(1)}, f32[2]{0:T(128)}, u32[]{:S(2)}) copy-start(f32[2]{0:T(128)} %log_step_ref.1) | copy-start | bytes 28
  1.5 20.9 %copy-start.19 = (f32[32]{0:T(128)S(1)}, f32[32]{0:T(128)}, u32[]{:S(2)}) copy-start(f32[32]{0:T(128)} %param.30) | copy-start | bytes 388
  22.4 14.1 %copy-start = (bf16[1024,2048]{1,0:T(8,128)(2,1)S(1)}, bf16[1024,2048]{1,0:T(8,128)(2,1)}, u32[]{:S(2)}) copy-start(bf16[1024,2048]{1,0:T(8,128)(2,1)} %w_out_ref.1) | copy-start | bytes 12582916
  22.4 14.1 %copy-start.13 = (f32[2048]{0:T(1024)S(1)}, f32[2048]{0:T(1024)}, u32[]{:S(2)}) copy-start(f32[2048]{0:T(1024)} %param.34) | copy-start | bytes 24580
  22.4 14.1 %copy-start.16 = (s32[64,2]{0,1:T(2,128)S(1)}, s32[64,2]{0,1:T(2,128)}, u32[]{:S(2)}) copy-start(s32[64,2]{0,1:T(2,128)} %param.35) | copy-start | bytes 1540
  22.4 14.1 %copy-start.17 = (f32[64,2]{0,1:T(2,128)S(1)}, f32[64,2]{0,1:T(2,128)}, u32[]{:S(2)}) copy-start(f32[64,2]{0,1:T(2,128)} %param.36) | copy-start | bytes 1540
  36.5 56.2 %copy-start.1 = (bf16[1,2048,256]{2,1,0:T(8,128)(2,1)S(1)}, bf16[1,2048,256]{2,1,0:T(8,128)(2,1)}, u32[]{:S(2)}) copy-start(bf16[1,2048,256]{2,1,0:T(8,128)(2,1)} %param.37) | copy-start | bytes 3145732
  36.5 56.2 %copy-start.2 = (bf16[1,2048,256]{2,1,0:T(8,128)(2,1)S(1)}, bf16[1,2048,256]{2,1,0:T(8,128)(2,1)}, u32[]{:S(2)}) copy-start(bf16[1,2048,256]{2,1,0:T(8,128)(2,1)} %param.38) | copy-start | bytes 3145732
  36.5 56.2 %copy-start.3 = (bf16[1,256,2048]{2,1,0:T(8,128)(2,1)S(1)}, bf16[1,256,2048]{2,1,0:T(8,128)(2,1)}, u32[]{:S(2)}) copy-start(bf16[1,256,2048]{2,1,0:T(8,128)(2,1)} %param.39) | copy-start | bytes 3145732

commit v6 on v5

--- a/solution.py
+++ b/solution.py
@@ -267,7 +267,6 @@
     for copy in copies:
         copy.start()
     pieces, _, share = piece_ref.shape
-    count, _, part = parts_ref.shape
     gate = upper = None
     for k in range(pieces):
         piece = piece_ref[k]
@@ -276,19 +275,11 @@
         gate = g if gate is None else gate + g
         upper = u if upper is None else upper + u
     hidden = (jax.nn.silu(gate) * upper).astype(BF16)
-    rows = hidden.shape[0]
-    low = lanes((rows, 128)) < 64
-    block = 64 * count
-    for m in range(part // 128):
-        value = dot(hidden, down_ref[:, 2 * m * block : (2 * m + 2) * block])
-        for k in range(count):
-            a = value[:, k // 2 * 128 : k // 2 * 128 + 128]
-            b = value[:, block + k // 2 * 128 : block + k // 2 * 128 + 128]
-            if k % 2:
-                joined = jnp.where(low, lane_roll(a, 64), b)
-            else:
-                joined = jnp.where(low, a, lane_roll(b, 64))
-            parts_ref[k, :, m * 128 : (m + 1) * 128] = joined.astype(BF16)
+    block = 8 * 64
+    for m in range(parts_ref.shape[0] * 64 // block):
+        value = dot(hidden, down_ref[:, m * block : (m + 1) * block]).T
+        for k in range(8):
+            parts_ref[8 * m + k] = value[k * 64 : (k + 1) * 64, :].astype(BF16)
     for copy in copies:
         copy.wait()
 
@@ -298,31 +289,19 @@
     for k in range(1, arrived_ref.shape[0]):
         total = total + arrived_ref[k].astype(F32)
     total = total.astype(BF16)
-    slots = total.shape[0]
+    slots = total.shape[1]
     halves = []
     for half in range(2):
         order = slot_of((slots // 2, slots), 0, capacity, half)
         one = jnp.ones(order.shape, F32)
         pick = jnp.where(order == lanes(order.shape), one, jnp.zeros_like(one)).astype(BF16)
-        halves.append(dot(pick, total))
-    first, second = halves
-    experts, rows, short, _ = out_ref.shape
-    low = lanes((slots // 2, 128)) < 64
-    for m in range(rows // 2):
-        a = first[:, m * 128 : (m + 1) * 128]
-        b = second[:, m * 128 : (m + 1) * 128]
-        even = jnp.where(low, a, lane_roll(b, 64)).astype(BF16)
-        odd = jnp.where(low, lane_roll(a, 64), b).astype(BF16)
-        out_ref[:, 2 * m] = even.reshape(experts, short, 128)
-        out_ref[:, 2 * m + 1] = odd.reshape(experts, short, 128)
+        halves.append(dot_nt(pick, total))
+    out_ref[...] = jnp.concatenate(halves, axis=1).astype(BF16).reshape(out_ref.shape)
 
 
 def combine_kernel(returned_ref, pick_ref, weight_ref, own_ref, out_ref):
-    experts, rows, short, _ = returned_ref.shape
-    returned = returned_ref[:, 0].astype(F32)
-    for k in range(1, rows):
-        returned = returned + returned_ref[:, k].astype(F32)
-    returned = returned.reshape(experts * short, 128).astype(BF16)
+    returned = returned_ref[...]
+    returned = returned.reshape(returned.shape[0] * returned.shape[1], 128)
     total = own_ref[:, :64]
     for k in range(2):
         picked = dot(pick_ref[2 * k], returned)[:, :64] + dot(pick_ref[2 * k + 1], returned)[:, 64:]
@@ -410,7 +389,7 @@
     parts, next_re, next_im = call(
         expert_kernel,
         (
-            sds((near, slots, far * local_width), BF16),
+            sds((tp_count, local_width, slots), BF16),
             sds(state_real.shape, F32),
             sds(state_real.shape, F32),
         ),
@@ -423,13 +402,11 @@
         hbm_outs=(1, 2),
         scratch=(pltpu.SemaphoreType.DMA((2,)),),
     )
-    arrived = exchange(parts, NEAR)
-    short = capacity // 2
+    arrived = exchange(parts, TP)
     results = call(
-        functools.partial(sum_kernel, capacity), sds((experts, far, short, 128), BF16), arrived
-    )
-    returned = exchange(results.reshape(experts * far, short, 128), ("ep", "yh"))
-    returned = returned.reshape(experts, far, short, 128)
+        functools.partial(sum_kernel, capacity), sds((experts, capacity // 2, 128), BF16), arrived
+    )
+    returned = exchange(results, "ep")
     layer_out = call(
         combine_kernel, sds((rows, local_width), BF16), returned, picks, weights, own
     )

time: 143 us -> 146 us (1.021)
  blocking collectives: 136 us -> 138 us
    all_to_all x6, blocking collectives: 136 us -> 138 us  [exchange(): return lax.all_to_all(parts, axis, split_axis=0, concat_axis=0, tiled=True)]
where the time goes in v6:
time: 146 us; the launch traced here: 145 us
  blocking collectives  138 us (95%)
  Pallas kernels  4.98 us (3%)
    all_to_all x6, blocking collectives, exchange(): return lax.all_to_all(parts, axis, split_axis=0, concat_axis=0, tiled=True)  138 us
    pallas_call x6, Pallas kernels, call(): pl.pallas_call(kernel, out_shape=out_shape, in_specs=specs, out_specs=out...  4.98 us

profile of v6, /device:TPU:1, one launch (start us, length us, event | category | flops | bytes accessed | tf_op | source)
XLA Modules:
  0.0 145.1 jit_solution(13716731309041709178)
XLA Ops:
  0.6 0.0 copy-start.6
  0.6 0.0 copy-start.5
  0.7 0.0 copy-start.4
  0.7 0.7 copy-done.7
  1.5 0.1 shard_map.211
  1.6 20.7 %all_to_all.30.arrived_ref = bf16[32,32,128]{2,1,0:T(8,128)(2,1)S(1)} all-to-all(bf16[32,32,128]{2,1,0:T(8,128)(2,1)S(1)} %shard_map.211), channel_id=1, replica_groups=mesh['ep'=32,'yh'=4,'yl'=2,'x'=4] {'yh','yl','x'}, dimensions={0} | all-to-all | bytes 524288 | tf_op jit(solution)/shard_map/all_to_all | solution.py:22
  22.4 0.0 copy-start
  22.4 0.0 copy-start.13
  22.4 0.0 copy-start.16
  22.4 0.0 copy-start.17
  22.4 1.4 shard_map.212
  23.8 12.7 %all_to_all.31.arrived_ref = bf16[32,16,128]{2,1,0:T(8,128)(2,1)S(1)} all-to-all(bf16[32,16,128]{2,1,0:T(8,128)(2,1)S(1)} %get-tuple-element.14), channel_id=1, replica_groups=mesh['ep'=32,'yh'=4,'yl'=2,'x'=4] {'yh','yl','x'}, dimensions={0} | all-to-all | bytes 262144 | tf_op jit(solution)/shard_map/all_to_all | solution.py:22
  36.5 0.0 copy-start.1
  36.5 0.0 copy-start.2
  36.5 0.0 copy-start.3
  36.5 1.1 shard_map.213
  37.7 39.5 %all_to_all.32 = bf16[32,8,256]{2,1,0:T(8,128)(2,1)S(1)} all-to-all(bf16[32,8,256]{2,1,0:T(8,128)(2,1)S(1)} %get-tuple-element.16), channel_id=1, replica_groups=mesh['ep'=32,'yh'=4,'yl'=2,'x'=4] {'ep'}, dimensions={0} | all-to-all | bytes 262144 | tf_op jit(solution)/shard_map/all_to_all | solution.py:22
  77.2 0.1 broadcast_in_dim.3
  77.3 15.4 %all_to_all.33.piece_ref = bf16[8,256,256]{2,1,0:T(8,128)(2,1)S(1)} all-to-all(bf16[8,256,256]{2,1,0:T(8,128)(2,1)S(1)} %broadcast_in_dim.3), channel_id=1, replica_groups=mesh['ep'=32,'yh'=4,'yl'=2,'x'=4] {'yl','x'}, dimensions={0} | all-to-all | bytes 2097152 | tf_op jit(solution)/shard_map/all_to_all | solution.py:22
  92.7 1.2 shard_map.214
  93.9 30.1 %all_to_all.34.arrived_ref = bf16[32,64,256]{2,1,0:T(8,128)(2,1)S(1)} all-to-all(bf16[32,64,256]{2,1,0:T(8,128)(2,1)S(1)} %get-tuple-element.19), channel_id=1, replica_groups=mesh['ep'=32,'yh'=4,'yl'=2,'x'=4] {'yh','yl','x'}, dimensions={0} | all-to-all | bytes 2097152 | tf_op jit(solution)/shard_map/all_to_all | solution.py:22
  124.0 0.4 shard_map.215
  124.3 20.0 %all_to_all.35.returned_ref = bf16[32,4,128]{2,1,0:T(4,128)(2,1)S(1)} all-to-all(bf16[32,4,128]{2,1,0:T(4,128)(2,1)S(1)} %shard_map.215), channel_id=1, replica_groups=mesh['ep'=32,'yh'=4,'yl'=2,'x'=4] {'ep'}, dimensions={0} | all-to-all | bytes 65536 | tf_op jit(solution)/shard_map/all_to_all | solution.py:22
  144.3 0.8 shard_map.216
  (29 shorter events, 0.1 us)
Async XLA Ops:
  0.6 21.6 %copy-start.6 = (f32[64,2,64]{2,1,0:T(2,128)S(1)}, f32[64,2,64]{2,1,0:T(2,128)}, u32[]{:S(2)}) copy-start(f32[64,2,64]{2,1,0:T(2,128)} %state_im_ref.1) | copy-start | bytes 98308
  0.6 21.6 %copy-start.5 = (f32[64,2,64]{2,1,0:T(2,128)S(1)}, f32[64,2,64]{2,1,0:T(2,128)}, u32[]{:S(2)}) copy-start(f32[64,2,64]{2,1,0:T(2,128)} %state_re_ref.1) | copy-start | bytes 98308
  0.7 21.6 %copy-start.4 = (bf16[2048,32]{0,1:T(8,128)(2,1)S(1)}, bf16[2048,32]{0,1:T(8,128)(2,1)}, u32[]{:S(2)}) copy-start(bf16[2048,32]{0,1:T(8,128)(2,1)} %param.22) | copy-start | bytes 393220
  0.7 0.8 copy-start.7
  1.4 20.9 %copy-start.8 = (f32[2,64,16]{1,2,0:T(8,128)S(1)}, f32[2,64,16]{1,2,0:T(8,128)}, u32[]{:S(2)}) copy-start(f32[2,64,16]{1,2,0:T(8,128)} %param.26) | copy-start | bytes 24580
  1.4 20.9 %copy-start.9 = (f32[2,64,16]{1,2,0:T(8,128)S(1)}, f32[2,64,16]{1,2,0:T(8,128)}, u32[]{:S(2)}) copy-start(f32[2,64,16]{1,2,0:T(8,128)} %param.27) | copy-start | bytes 24580
  1.4 20.9 %copy-start.10 = (f32[2,16,64]{2,1,0:T(8,128)S(1)}, f32[2,16,64]{2,1,0:T(8,128)}, u32[]{:S(2)}) copy-start(f32[2,16,64]{2,1,0:T(8,128)} %out_re_ref.1) | copy-start | bytes 24580
  1.4 20.9 %copy-start.11 = (f32[2,16,64]{2,1,0:T(8,128)S(1)}, f32[2,16,64]{2,1,0:T(8,128)}, u32[]{:S(2)}) copy-start(f32[2,16,64]{2,1,0:T(8,128)} %out_im_ref.1) | copy-start | bytes 24580
  1.4 20.9 %copy-start.12 = (f32[2048]{0:T(1024)S(1)}, f32[2048]{0:T(1024)}, u32[]{:S(2)}) copy-start(f32[2048]{0:T(1024)} %param.21) | copy-start | bytes 24580
  1.4 20.9 %copy-start.14 = (f32[2,64]{1,0:T(2,128)S(1)}, f32[2,64]{1,0:T(2,128)}, u32[]{:S(2)}) copy-start(f32[2,64]{1,0:T(2,128)} %decay_ref.1) | copy-start | bytes 1540
  1.5 20.9 %copy-start.15 = (f32[2,64]{1,0:T(2,128)S(1)}, f32[2,64]{1,0:T(2,128)}, u32[]{:S(2)}) copy-start(f32[2,64]{1,0:T(2,128)} %freq_ref.1) | copy-start | bytes 1540
  1.5 20.9 %copy-start.18 = (f32[2]{0:T(128)S(1)}, f32[2]{0:T(128)}, u32[]{:S(2)}) copy-start(f32[2]{0:T(128)} %log_step_ref.1) | copy-start | bytes 28
  1.5 20.9 %copy-start.19 = (f32[32]{0:T(128)S(1)}, f32[32]{0:T(128)}, u32[]{:S(2)}) copy-start(f32[32]{0:T(128)} %param.30) | copy-start | bytes 388
  22.4 14.1 %copy-start = (bf16[1024,2048]{1,0:T(8,128)(2,1)S(1)}, bf16[1024,2048]{1,0:T(8,128)(2,1)}, u32[]{:S(2)}) copy-start(bf16[1024,2048]{1,0:T(8,128)(2,1)} %w_out_ref.1) | copy-start | bytes 12582916
  22.4 14.1 %copy-start.13 = (f32[2048]{0:T(1024)S(1)}, f32[2048]{0:T(1024)}, u32[]{:S(2)}) copy-start(f32[2048]{0:T(1024)} %param.34) | copy-start | bytes 24580
  22.4 14.1 %copy-start.16 = (s32[64,2]{0,1:T(2,128)S(1)}, s32[64,2]{0,1:T(2,128)}, u32[]{:S(2)}) copy-start(s32[64,2]{0,1:T(2,128)} %param.35) | copy-start | bytes 1540
  22.4 14.1 %copy-start.17 = (f32[64,2]{0,1:T(2,128)S(1)}, f32[64,2]{0,1:T(2,128)}, u32[]{:S(2)}) copy-start(f32[64,2]{0,1:T(2,128)} %param.36) | copy-start | bytes 1540
  36.5 56.2 %copy-start.1 = (bf16[1,2048,256]{2,1,0:T(8,128)(2,1)S(1)}, bf16[1,2048,256]{2,1,0:T(8,128)(2,1)}, u32[]{:S(2)}) copy-start(bf16[1,2048,256]{2,1,0:T(8,128)(2,1)} %param.37) | copy-start | bytes 3145732
  36.5 56.2 %copy-start.2 = (bf16[1,2048,256]{2,1,0:T(8,128)(2,1)S(1)}, bf16[1,2048,256]{2,1,0:T(8,128)(2,1)}, u32[]{:S(2)}) copy-start(bf16[1,2048,256]{2,1,0:T(8,128)(2,1)} %param.38) | copy-start | bytes 3145732
  36.5 56.2 %copy-start.3 = (bf16[1,256,2048]{2,1,0:T(8,128)(2,1)S(1)}, bf16[1,256,2048]{2,1,0:T(8,128)(2,1)}, u32[]{:S(2)}) copy-start(bf16[1,256,2048]{2,1,0:T(8,128)(2,1)} %param.39) | copy-start | bytes 3145732
